TPU v7x, 32 devices: a whole 2x2x4 slice. The times are simulated.
32 devices in a mesh: sp: 16 (over z, y, x), tp: 2 (over core).
Axes of the slice: x: 2, y: 2, z: 4, core: 2. Of those that a mesh axis runs over, the one named last changes fastest.
Arguments:
- hidden_in: bfloat16 [8192, 2048], P('sp'), may hold values from -64 to 64
- pre_gain: float32 [2048], replicated, may hold values from 0.1 to 1.9
- query_proj: bfloat16 [2048, 2048], P(None, 'tp'), may hold values from -2 to 2
- key_proj: bfloat16 [2048, 2048], P('sp', 'tp'), may hold values from -2 to 2
- value_proj: bfloat16 [2048, 2048], P('sp', 'tp'), may hold values from -0.125 to 0.125
- out_proj: bfloat16 [2048, 2048], P('tp'), may hold values from -0.125 to 0.125
- post_gain: float32 [2048], replicated, may hold values from 0.1 to 1.9
Outputs:
- layer_out: bfloat16 [8192, 2048], P(('sp', 'tp'))
- log_weight: float32 [32, 8192], P('tp', 'sp')
All inputs are finite; a program needn't handle non-finite values.
Results may differ from a plain program's by a relative error of at most 0.018.
The roundings to bfloat16 on the way count: a program that leaves them out, or rounds other values in their place, can miss the bound.
Values may be sent and summed in bfloat16 or wider, within the bound.
A program may use at most 128 MiB of HBM per device.

v0:
```python
import functools

import jax
import jax.numpy as jnp
from jax import lax
from jax.experimental import pallas as pl
from jax.experimental.pallas import tpu as pltpu
from jax.sharding import PartitionSpec as P

HEAD_DIM = 64
SPAN = 128
EPS = 1e-06
ROPE_BASE = 10000.0
WIDE = 16
LANES = 128
MESH = pl.DeviceIdType.MESH
ANY = pl.BlockSpec(memory_space=pl.ANY)
NEG = -1e30


def greet(peers):
    barrier = pltpu.get_barrier_semaphore()
    for peer in peers:
        pl.semaphore_signal(barrier, inc=1, device_id=peer, device_id_type=MESH)
    pl.semaphore_wait(barrier, len(peers))


def remote(src, dst, send, recv, peer):
    return pltpu.make_async_remote_copy(
        src_ref=src, dst_ref=dst, send_sem=send, recv_sem=recv, device_id=peer, device_id_type=MESH
    )


def group_of(mesh, width):
    for size in (4, 2):
        if mesh.shape["sp"] % size == 0 and width % (size * LANES) == 0:
            return size
    return 1


def gather_kernel(n_sp, group, hid_ref, wk_ref, wv_ref, hid_out, wk_out, wv_out, hs, hr, fs, fr, ws, wr, local):
    s = lax.axis_index("sp")
    t = lax.axis_index("tp")
    rows = hid_ref.shape[0]
    half_rows = rows // 2
    depth, width = wk_ref.shape
    part = width // group
    c = lax.rem(s, group)
    base = s - c
    half = lax.rem(t, 2)
    sibling = (s, t + 1 - 2 * half)
    near = [base + lax.rem(c + k, group) for k in range(1, group)]
    far = [lax.rem(s + k * group, n_sp) for k in range(1, n_sp // group)]
    greet([(peer, t) for peer in near + far] + [sibling])
    mine = pl.ds(pl.multiple_of(half * half_rows, half_rows), half_rows)

    pairs = ((wk_ref, wk_out), (wv_ref, wv_out))
    into = pl.ds(pl.multiple_of(s * depth, depth), depth)
    cols = pl.ds(pl.multiple_of(c * part, LANES), part)
    kept = [
        pltpu.make_async_copy(src.at[:, cols], dst.at[into], local.at[j])
        for j, (src, dst) in enumerate(pairs)
    ]
    for copy in kept:
        copy.start()
    weights = []
    for k, peer in enumerate(near):
        cols = pl.ds(pl.multiple_of((peer - base) * part, LANES), part)
        for j, (src, dst) in enumerate(pairs):
            weights.append(remote(src.at[:, cols], dst.at[into], ws.at[2 * k + j], wr.at[2 * k + j], (peer, t)))
            weights[-1].start()
    copies = []
    for k, peer in enumerate(near):
        copies.append(remote(hid_ref.at[mine], hid_out.at[c, mine], hs.at[k], hr.at[k], (peer, t)))
        copies[-1].start()
    own = remote(hid_ref, hid_out.at[c], hs.at[group - 1], hr.at[group - 1], sibling)
    own.start()
    for copy in kept + weights:
        copy.wait()
    slot = pl.ds(pl.multiple_of(base * depth, depth), group * depth)
    passed = []
    for k, peer in enumerate(far):
        for j, (_, dst) in enumerate(pairs):
            at = 2 * (group - 1 + k) + j
            passed.append(remote(dst.at[slot], dst.at[slot], ws.at[at], wr.at[at], (peer, t)))
            passed[-1].start()
    forwards = []
    for k in range(1, group):
        copies[k - 1].wait_recv()
        slot = hid_out.at[lax.rem(c + group - k, group), mine]
        forwards.append(remote(slot, slot, fs.at[k - 1], fr.at[k - 1], sibling))
        forwards[-1].start()
    for copy in copies:
        copy.wait_send()
    for copy in forwards + passed + [own]:
        copy.wait()


def gather(mesh, group, hidden, key_proj, value_proj):
    n_sp = mesh.shape["sp"]
    depth, width = key_proj.shape
    part = width // group
    dma = pltpu.SemaphoreType.DMA
    weight = jax.ShapeDtypeStruct((n_sp * depth, part), key_proj.dtype)
    return pl.pallas_call(
        functools.partial(gather_kernel, n_sp, group),
        out_shape=(jax.ShapeDtypeStruct((group,) + hidden.shape, hidden.dtype), weight, weight),
        in_specs=[ANY] * 3,
        out_specs=(ANY,) * 3,
        scratch_shapes=[
            dma((group,)), dma((group,)), dma((group,)), dma((group,)),
            dma((2 * n_sp,)), dma((2 * n_sp,)), dma((2,)),
        ],
        compiler_params=pltpu.CompilerParams(collective_id=0, has_side_effects=True),
        name="gather_blocks",
    )(hidden, key_proj, value_proj)


def project_kernel(part, hid_ref, gain_ref, wq_ref, wk_ref, wv_ref, cos_ref, sin_ref, nat_ref, res_ref, scr):
    x = hid_ref[...].astype(jnp.float32)
    normed = x * lax.rsqrt(jnp.mean(x * x, axis=-1, keepdims=True) + EPS) * gain_ref[...]
    normed = normed.astype(jnp.bfloat16)
    rows = x.shape[0]
    front = lax.rem(lax.broadcasted_iota(jnp.int32, (rows, LANES), 1), HEAD_DIM) < HEAD_DIM // 2
    for j, w_ref in enumerate((wq_ref, wk_ref, wv_ref)):
        out = jnp.dot(normed, w_ref[...], preferred_element_type=jnp.float32)
        for i in range(part // LANES):
            u = out[:, i * LANES:(i + 1) * LANES]
            if j < 2:
                swapped = jnp.where(
                    front,
                    pltpu.roll(u, LANES - HEAD_DIM // 2, 1),
                    pltpu.roll(u, HEAD_DIM // 2, 1),
                )
                u = u * cos_ref[...] + swapped * sin_ref[...]
            if j == 0:
                u = u * HEAD_DIM ** (-0.5)
            scr[j * (part // LANES) + i] = u
    for i in range(3 * part // LANES):
        cols = pl.ds(i * LANES, LANES)
        nat_ref[:, cols] = scr[i].astype(jnp.bfloat16)
        for r in range(WIDE):
            res_ref[r, :, cols] = scr[i, pl.ds(r, rows // WIDE, stride=WIDE), :].astype(jnp.bfloat16)


def project(hid, gain, wq, wk, wv, cos_part, sin_part):
    rows, depth = hid.shape
    part = wk.shape[1]
    block = 256
    whole = pl.BlockSpec((depth, part), lambda i: (0, 0))
    table = pl.BlockSpec((block, LANES), lambda i: (i, 0))
    return pl.pallas_call(
        functools.partial(project_kernel, part),
        grid=(rows // block,),
        out_shape=(
            jax.ShapeDtypeStruct((rows, 3 * part), jnp.bfloat16),
            jax.ShapeDtypeStruct((WIDE, rows // WIDE, 3 * part), jnp.bfloat16),
        ),
        in_specs=[
            pl.BlockSpec((block, depth), lambda i: (i, 0)),
            pl.BlockSpec((1, depth), lambda i: (0, 0)),
            whole, whole, whole, table, table,
        ],
        out_specs=(
            pl.BlockSpec((block, 3 * part), lambda i: (i, 0)),
            pl.BlockSpec((WIDE, block // WIDE, 3 * part), lambda i: (0, i, 0)),
        ),
        scratch_shapes=[pltpu.VMEM((3 * part // LANES, block, LANES), jnp.float32)],
        compiler_params=pltpu.CompilerParams(vmem_limit_bytes=50 * 1024 * 1024),
        cost_estimate=pl.CostEstimate(flops=6 * rows * depth * part, bytes_accessed=2 * rows * depth, transcendentals=0),
        name="project_rows",
    )(hid, gain, wq, wk, wv, cos_part, sin_part)


def attend_kernel(
    n_sp, group, behind, pairs,
    nat_ref, res_ref, qn, kn, vn, qr, kr, vr,
    out_ref, lw_ref,
    kx_all, vx_all, kw_all, vw_all, acc1, m1, l1, acc4, m4, l4, acc16, m16, l16, b1, b4, b16, send, recv,
):
    rows = qn.shape[0]
    steps = rows // WIDE
    block = min(SPAN, steps)
    g = lax.axis_index("sp") // group
    f32 = jnp.float32
    s = lax.axis_index("sp")
    t = lax.axis_index("tp")
    p = pl.program_id(0)
    after = [lax.rem(s + b * group, n_sp) for b in range(1, behind + 1)]
    before = [lax.rem(s + n_sp - b * group, n_sp) for b in range(1, behind + 1)]
    last = pl.ds(rows - SPAN, SPAN)

    def early(pair):
        copies = []
        for j, (ref, first) in enumerate(((kw_all, pairs), (vw_all, 2 * pairs))):
            cols = pl.ds(pl.multiple_of((first + pair) * LANES, LANES), LANES)
            copies.append(remote(
                nat_ref.at[last, cols], ref.at[pair, pl.ds(0, SPAN)], send.at[pair, j], recv.at[pair, j], (after[0], t)
            ))
        return copies

    def late(pair):
        copies = []
        for j, (ref, first) in enumerate(((kx_all, pairs), (vx_all, 2 * pairs))):
            cols = pl.ds(pl.multiple_of((first + pair) * LANES, LANES), LANES)
            for b in range(1, behind + 1):
                at = 2 * b + j
                copies.append(remote(
                    res_ref.at[:, :, cols],
                    ref.at[pair, :, pl.ds((behind - b) * steps, steps)],
                    send.at[pair, at], recv.at[pair, at], (after[b - 1], t),
                ))
        return copies

    @pl.when(p == 0)
    def _():
        greet([(peer, t) for peer in after + before])
        for pair in range(pairs):
            for copy in early(pair):
                copy.start()
        for pair in range(pairs):
            for copy in late(pair):
                copy.start()

    kx, vx, kw, vw = (ref.at[p] for ref in (kx_all, vx_all, kw_all, vw_all))
    kx[:, SPAN:, :] = kr[...]
    vx[:, SPAN:, :] = vr[...]
    kw[SPAN:, :] = kn[...]
    vw[SPAN:, :] = vn[...]

    def put_bias(ref, near, count, first_of):
        shape = ref.shape[1:]
        a = lax.broadcasted_iota(jnp.int32, shape, 0)
        b = lax.broadcasted_iota(jnp.int32, shape, 1)
        distance, place = near(a, b)
        band = (distance >= 0) & (distance <= SPAN)
        ref[0] = jnp.where(band & (place + first_of >= 0), 0.0, NEG).astype(f32)
        ref[1] = jnp.where(band, 0.0, NEG).astype(f32)

    def plain(a, b):
        return a + SPAN - b, b - SPAN

    def woven(a, b):
        return 4 * (a % 32 + 32 - b % 64) + a // 32 - b // 64, b % 64 - 32

    put_bias(b1, plain, 0, g * rows)
    put_bias(b16, plain, 0, g * steps)
    put_bias(b4, woven, 0, g * steps)

    def tile(q, k, v, bias):
        count = q.shape[0]
        low = lax.broadcasted_iota(jnp.int32, (count, LANES), 1) < HEAD_DIM
        low_q = low.astype(f32).astype(jnp.bfloat16)
        both = jnp.concatenate([q * low_q, q * (1 - low_q)], axis=0)
        s = lax.dot_general(both, k, (((1,), (1,)), ((), ())), preferred_element_type=f32)
        s = s + jnp.concatenate([bias, bias], axis=0)
        m = jnp.max(s, axis=-1, keepdims=True)
        p = jnp.exp(s - m).astype(jnp.bfloat16)
        o = jnp.dot(p, jnp.concatenate([v, jnp.ones_like(v)], axis=1), preferred_element_type=f32)
        wide_m = jnp.broadcast_to(m, (2 * count, LANES))
        return (
            jnp.where(low, o[:count, :LANES], o[count:, :LANES]),
            jnp.where(low, wide_m[:count], wide_m[count:]),
            jnp.where(low, o[:count, LANES:], o[count:, LANES:]),
        )

    blocks16 = steps // block

    def step16(idx, _):
        r = idx // blocks16
        i = idx % blocks16
        at = pl.multiple_of(i * block, block)
        keys = pl.ds(at, block + SPAN)
        got = tile(qr[r, pl.ds(at, block), :], kx[r, keys, :], vx[r, keys, :], b16[jnp.minimum(i, 1)])
        for ref, value in zip((acc16, m16, l16), got):
            ref[pl.ds(r + WIDE * at, block, stride=WIDE), :] = value
        return 0

    blocks4 = steps // 32

    def step4(r, i):
        at = pl.multiple_of(i * 32, 32) if not isinstance(i, int) else i * 32
        keys = pl.ds(pl.multiple_of(at + SPAN - 32, 32) if not isinstance(i, int) else at + SPAN - 32, 64)
        got = tile(
            jnp.concatenate([qr[r + 4 * j, pl.ds(at, 32), :] for j in range(4)], axis=0),
            jnp.concatenate([kx[r + 4 * j, keys, :] for j in range(4)], axis=0),
            jnp.concatenate([vx[r + 4 * j, keys, :] for j in range(4)], axis=0),
            b4[0 if isinstance(i, int) else 1],
        )
        for ref, value in zip((acc4, m4, l4), got):
            for j in range(4):
                ref[pl.ds(r + 4 * j + WIDE * at, 32, stride=WIDE), :] = value[j * 32:(j + 1) * 32]
        return 0


    def step1(i, _):
        at = pl.multiple_of(i * SPAN, SPAN)
        here = pl.ds(at, SPAN)
        keys = pl.ds(at, 2 * SPAN)
        got = tile(qn[here, :], kw[keys, :], vw[keys, :], b1[jnp.minimum(i, 1)])
        for ref, value in zip((acc1, m1, l1), got):
            ref[here, :] = value
        return 0

    def merge(i, _):
        here = pl.ds(pl.multiple_of(i * SPAN, SPAN), SPAN)
        tops = (m1[here, :], m4[here, :], m16[here, :])
        top = jnp.maximum(tops[0], jnp.maximum(tops[1], tops[2]))
        e1, e4, e16 = (jnp.exp(x - top) for x in tops)
        total = l1[here, :] * e1 + l4[here, :] * e4 + l16[here, :] * e16
        mixed = acc1[here, :] * e1 + acc4[here, :] * e4 + acc16[here, :] * e16
        out_ref[here, :] = (mixed / total).astype(out_ref.dtype)
        turned = jnp.transpose(top + jnp.log(total))
        lw_ref[0, 0:1, here] = turned[0:1]
        lw_ref[0, 1:2, here] = turned[HEAD_DIM:HEAD_DIM + 1]
        return 0

    if blocks4 > 1:
        lax.fori_loop(
            0, 4 * (blocks4 - 1),
            lambda idx, _: step4(idx // (blocks4 - 1), idx % (blocks4 - 1) + 1), 0, unroll=2,
        )
    for copy in early(p):
        copy.wait()
    lax.fori_loop(0, rows // SPAN, step1, 0, unroll=2)
    for copy in late(p):
        copy.wait()
    lax.fori_loop(0, 4, lambda r, _: step4(r, 0), 0, unroll=2)
    lax.fori_loop(0, WIDE * blocks16, step16, 0, unroll=2)
    lax.fori_loop(0, rows // SPAN, merge, 0, unroll=2)


def attend(mesh, group, behind, nat, res):
    rows, part3 = nat.shape
    part = part3 // 3
    pairs = part // LANES
    steps = rows // WIDE
    block = min(SPAN, steps)

    def nat_spec(count, off):
        return pl.BlockSpec((count, LANES), lambda p: (0, p + off))

    def res_spec(off):
        return pl.BlockSpec((WIDE, steps, LANES), lambda p: (0, 0, p + off))

    f32 = jnp.float32
    state = pltpu.VMEM((rows, LANES), f32)
    return pl.pallas_call(
        functools.partial(attend_kernel, mesh.shape["sp"], group, behind, pairs),
        grid=(pairs,),
        out_shape=(
            jax.ShapeDtypeStruct((rows, part), jnp.bfloat16),
            jax.ShapeDtypeStruct((pairs, 2, rows), f32),
        ),
        in_specs=[
            ANY, ANY,
            nat_spec(rows, 0), nat_spec(rows, pairs), nat_spec(rows, 2 * pairs),
            res_spec(0), res_spec(pairs), res_spec(2 * pairs),
        ],
        out_specs=(
            pl.BlockSpec((rows, LANES), lambda p: (0, p)),
            pl.BlockSpec((1, 2, rows), lambda p: (p, 0, 0)),
        ),
        scratch_shapes=[
            pltpu.VMEM((pairs, WIDE, SPAN + steps, LANES), jnp.bfloat16),
            pltpu.VMEM((pairs, WIDE, SPAN + steps, LANES), jnp.bfloat16),
            pltpu.VMEM((pairs, SPAN + rows, LANES), jnp.bfloat16),
            pltpu.VMEM((pairs, SPAN + rows, LANES), jnp.bfloat16),
            state, state, state, state, state, state, state, state, state,
            pltpu.VMEM((2, SPAN, 2 * SPAN), f32),
            pltpu.VMEM((2, SPAN, 2 * SPAN), f32),
            pltpu.VMEM((2, block, block + SPAN), f32),
            pltpu.SemaphoreType.DMA((pairs, 2 * behind + 2)),
            pltpu.SemaphoreType.DMA((pairs, 2 * behind + 2)),
        ],
        compiler_params=pltpu.CompilerParams(
            vmem_limit_bytes=56 * 1024 * 1024, collective_id=1, has_side_effects=True
        ),
        cost_estimate=pl.CostEstimate(flops=6 * rows * 512 * part, bytes_accessed=8 * rows * part, transcendentals=0),
        name="attend_windows",
    )(nat, res, nat, nat, nat, res, res, res)


def return_kernel(group, rows, att_ref, lw_ref, att_out, lw_out, send, recv, local):
    s = lax.axis_index("sp")
    t = lax.axis_index("tp")
    part = att_ref.shape[1]
    c = lax.rem(s, group)
    base = s - c
    peers = [lax.rem(c + k, group) for k in range(1, group)]
    if group > 1:
        greet([(base + peer, t) for peer in peers])
    cols = pl.ds(pl.multiple_of(c * part, LANES), part)

    def pieces(peer):
        span = pl.ds(pl.multiple_of(peer * rows, rows), rows)
        return ((att_ref.at[span], att_out.at[:, cols]), (lw_ref.at[:, :, span], lw_out.at[c]))

    copies = []
    for k, peer in enumerate(peers):
        for j, (src, dst) in enumerate(pieces(peer)):
            copies.append(remote(src, dst, send.at[2 * k + j], recv.at[2 * k + j], (base + peer, t)))
    for j, (src, dst) in enumerate(pieces(c)):
        copies.append(pltpu.make_async_copy(src, dst, local.at[j]))
    for copy in copies:
        copy.start()
    for copy in copies:
        copy.wait()


def give_back(mesh, group, att, lw):
    rows = att.shape[0] // group
    part = att.shape[1]
    pairs = part // LANES
    dma = pltpu.SemaphoreType.DMA
    return pl.pallas_call(
        functools.partial(return_kernel, group, rows),
        out_shape=(
            jax.ShapeDtypeStruct((rows, part * group), att.dtype),
            jax.ShapeDtypeStruct((group, pairs, 2, rows), lw.dtype),
        ),
        in_specs=[ANY] * 2,
        out_specs=(ANY,) * 2,
        scratch_shapes=[dma((2 * group,)), dma((2 * group,)), dma((2,))],
        compiler_params=pltpu.CompilerParams(
            collective_id=2 if group > 1 else None, has_side_effects=True
        ),
        name="give_back",
    )(att, lw)


def swap_kernel(n_tp, part_ref, out_ref, send, recv):
    s = lax.axis_index("sp")
    t = lax.axis_index("tp")
    peers = [lax.rem(t + k, n_tp) for k in range(1, n_tp)]
    greet([(s, peer) for peer in peers])
    copies = [
        remote(part_ref.at[peer], out_ref.at[k], send.at[k], recv.at[k], (s, peer))
        for k, peer in enumerate(peers)
    ]
    for copy in copies:
        copy.start()
    for copy in copies:
        copy.wait()


def swap(mesh, partial):
    n_tp = mesh.shape["tp"]
    dma = pltpu.SemaphoreType.DMA
    return pl.pallas_call(
        functools.partial(swap_kernel, n_tp),
        out_shape=jax.ShapeDtypeStruct((n_tp - 1,) + partial.shape[1:], partial.dtype),
        in_specs=[ANY],
        out_specs=ANY,
        scratch_shapes=[dma((n_tp,)), dma((n_tp,))],
        compiler_params=pltpu.CompilerParams(collective_id=3, has_side_effects=True),
        name="swap_partials",
    )(partial)


def tables(rows, offset):
    half = HEAD_DIM // 2
    frequency = ROPE_BASE ** (-(jnp.arange(half, dtype=jnp.float32) * 2.0 / HEAD_DIM))
    positions = (offset + jnp.arange(rows, dtype=jnp.int32)).astype(jnp.float32)
    angles = positions[:, None] * frequency[None, :]
    cos_part = jnp.cos(angles)
    sin_part = jnp.sin(angles)
    return (
        jnp.concatenate([cos_part] * 4, axis=1),
        jnp.concatenate([-sin_part, sin_part] * 2, axis=1),
    )


def body(mesh, hidden_in, pre_gain, query_proj, key_proj, value_proj, out_proj, post_gain):
    rows, depth = hidden_in.shape
    width = query_proj.shape[1]
    n_tp = mesh.shape["tp"]
    group = group_of(mesh, width)
    part = width // group
    s = lax.axis_index("sp")
    t = lax.axis_index("tp")
    c = lax.rem(s, group)
    all_rows = rows * group
    behind = -(-(WIDE * SPAN) // all_rows)
    hid, wk, wv = gather(mesh, group, hidden_in, key_proj, value_proj)
    wq = lax.dynamic_slice_in_dim(query_proj, c * part, part, axis=1)
    cos_part, sin_part = tables(all_rows, (s - c) * rows)
    nat, res = project(
        hid.reshape(all_rows, depth), pre_gain[None, :], wq, wk, wv, cos_part, sin_part
    )
    att, lw = attend(mesh, group, behind, nat, res)
    attended, log_weight = give_back(mesh, group, att, lw)
    partial = jnp.dot(attended, out_proj, preferred_element_type=jnp.float32).astype(jnp.bfloat16)
    partial = partial.reshape(n_tp, rows // n_tp, depth)
    others = swap(mesh, partial)
    own = lax.dynamic_index_in_dim(partial, t, 0, keepdims=False)
    summed = own.astype(jnp.float32) + jnp.sum(others.astype(jnp.float32), axis=0)
    scale = lax.rsqrt(jnp.mean(summed * summed, axis=-1, keepdims=True) + EPS)
    layer_out = (summed * scale * post_gain).astype(jnp.bfloat16)
    return (layer_out, log_weight.reshape(width // HEAD_DIM, rows))


def solution(mesh):
    placed = (P("sp", None), P(), P(None, "tp"), P("sp", "tp"), P("sp", "tp"), P("tp", None), P())
    return jax.shard_map(
        functools.partial(body, mesh),
        mesh=mesh,
        in_specs=placed,
        out_specs=(P(("sp", "tp"), None), P("tp", "sp")),
        check_vma=False,
    )
```

profile of v0, /device:TPU:9, one launch (start us, length us, event | category | flops | bytes accessed | tf_op | source)
XLA Modules:
  0.0 177.3 jit_solution(10043821680578424435)
XLA Ops:
  0.7 1.3 constant_dynamic-slice_fusion.wq_ref
  2.0 3.7 %fusion.3 = (f32[2048,32]{1,0:T(8,128)S(1)}, f32[2048,32]{1,0:T(8,128)S(1)}, f32[2048,32]{1,0:T(8,128)S(1)}) fusion(f32[32]{0:T(128)S(1)} %negate_power_fusion, f32[2048]{0:T(1024)S(1)} %add_convert_fusion), kind=kLoop, calls=%fused_computation.11 | loop fusion | flops 131072 | bytes 794752 | tf_op jit(solution)/shard_map/neg | solution.py:470
  5.7 3.0 %pad_maximum_fusion = (f32[2048,128]{1,0:T(8,128)}, f32[2048,128]{1,0:T(8,128)}) fusion(f32[2048,32]{1,0:T(8,128)S(1)} %get-tuple-element.22, f32[2048,32]{1,0:T(8,128)S(1)} %get-tuple-element.21, f32[2048,32]{1,0:T(8,128)S(1)} %get-tuple-element.20), kind=kLoop, calls=%fused_computation.9 | loop fusion | flops 1572864 | bytes 2883584 | tf_op jit(solution)/shard_map/concatenate | solution.py:469
  8.7 0.0 copy-start.2
  8.7 60.8 %gather_blocks.1 = (bf16[4,512,2048]{2,1,0:T(8,128)(2,1)}, bf16[2048,256]{1,0:T(8,128)(2,1)}, bf16[2048,256]{1,0:T(8,128)(2,1)}) custom-call(bf16[512,2048]{1,0:T(8,128)(2,1)} %hid_ref.1, bf16[128,1024]{1,0:T(8,128)(2,1)} %wk_ref.1, bf16[128,1024]{1,0:T(8,128)(2,1)} %wv_ref.1), custom_call_target="tpu_custom_call" | custom-call | tf_op jit(solution)/shard_map/gather_blocks/pallas_call | solution.py:105
  69.5 0.0 copy-done.2
  69.6 0.0 copy-start
  69.6 1.2 copy-done
  70.8 0.0 copy-start.1
  70.8 1.2 copy-done.1
  72.0 14.6 %project_rows.1 = (bf16[2048,768]{1,0:T(8,128)(2,1)}, bf16[16,128,768]{2,1,0:T(8,128)(2,1)}) custom-call(bf16[2048,2048]{1,0:T(8,128)(2,1)} %bitcast.18, f32[1,2048]{1,0:T(1,128)S(1)} %bitcast.14, bf16[2048,256]{1,0:T(8,128)(2,1)S(1)} %constant_dynamic-slice_fusion.wq_ref, bf16[2048,256]{1,0:T(8,128)(2,1)S(1)} %copy-done, bf16[2048,256]{1,0:T(8,128)(2,1)S(1)} %copy-done.1, ...), custom_call_target="tpu_custom_call" | custom-call | flops 6442450944 | bytes 8388608 | tf_op jit(solution)/shard_map/project_rows/pallas_call | solution.py:152
  86.6 61.0 %attend_windows.1 = (bf16[2048,256]{1,0:T(8,128)(2,1)}, f32[2,2,2048]{2,1,0:T(2,128)}) custom-call(bf16[2048,768]{1,0:T(8,128)(2,1)} %get-tuple-element.14.nat_ref.qn.kn.vn, bf16[16,128,768]{2,1,0:T(8,128)(2,1)} %get-tuple-element.15.res_ref.qr.kr.vr, bf16[2048,768]{1,0:T(8,128)(2,1)} %get-tuple-element.14.nat_ref.qn.kn.vn, ...), custom_call_target="tpu_custom_call" | custom-call | flops 1610612736 | bytes 4194304 | tf_op jit(solution)/shard_map/attend_windows/pallas_call | solution.py:348
  147.6 14.3 %give_back.1 = (bf16[512,1024]{1,0:T(8,128)(2,1)}, f32[4,2,2,512]{3,2,1,0:T(2,128)}) custom-call(bf16[2048,256]{1,0:T(8,128)(2,1)} %get-tuple-element.16.att_ref, f32[2,2,2048]{2,1,0:T(2,128)} %get-tuple-element.17.lw_ref), custom_call_target="tpu_custom_call" | custom-call | tf_op jit(solution)/shard_map/give_back/pallas_call | solution.py:416
  161.9 1.4 reshape.38
  163.3 6.2 %convolution_convert_fusion = bf16[512,2048]{1,0:T(8,128)(2,1)} fusion(bf16[512,1024]{1,0:T(8,128)(2,1)} %get-tuple-element.18, bf16[1024,2048]{1,0:T(8,128)(2,1)} %param.12), kind=kOutput, calls=%fused_computation | convolution fusion | flops 2148532224 | bytes 7340032 | tf_op jit(solution)/shard_map/dot_general | solution.py:493
  169.5 0.0 copy-start.4
  169.5 0.0 copy-start.5
  169.5 4.5 %swap_partials.1 = bf16[1,256,2048]{2,1,0:T(8,128)(2,1)} custom-call(bf16[2,256,2048]{2,1,0:T(8,128)(2,1)} %bitcast.15), custom_call_target="tpu_custom_call" | custom-call | tf_op jit(solution)/shard_map/swap_partials/pallas_call | solution.py:450
  174.0 0.0 copy-done.4
  174.0 0.0 copy-start.3
  174.0 1.7 fusion
  175.8 0.0 copy-done.5
  175.8 0.0 copy-done.3
  175.8 1.5 fusion.2
  (3 shorter events, 0.0 us)
Async XLA Ops:
  8.7 60.8 %copy-start.2 = (f32[2048]{0:T(1024)S(1)}, f32[2048]{0:T(1024)}, u32[]{:S(2)}) copy-start(f32[2048]{0:T(1024)} %param.8) | copy-start | bytes 24580
  69.6 1.2 copy-start
  70.8 1.2 copy-start.1
  169.5 4.5 %copy-start.4 = (bf16[512,2048]{1,0:T(8,128)(2,1)S(1)}, bf16[512,2048]{1,0:T(8,128)(2,1)}, u32[]{:S(2)}) copy-start(bf16[512,2048]{1,0:T(8,128)(2,1)} %convolution_convert_fusion) | copy-start | bytes 6291460
  169.5 6.3 %copy-start.5 = (f32[2048]{0:T(1024)S(1)}, f32[2048]{0:T(1024)}, u32[]{:S(2)}) copy-start(f32[2048]{0:T(1024)} %param.13) | copy-start | bytes 24580
  174.0 1.8 copy-start.3
where the time goes:
time: 180 us; the launch traced here: 177 us
  Pallas kernels  155 us (86%)
  other arithmetic  9.98 us (6%)
  matrix products  6.19 us (3%)
  local copies, waits for them, and re-layouts  5.15 us (3%)
    pallas_call x1, Pallas kernels, attend(): pl.pallas_call(functools.partial(attend_kernel, mesh.shape['sp'], group,...  61 us
    pallas_call x1, Pallas kernels, gather(): pl.pallas_call(functools.partial(gather_kernel, n_sp, group), out_shape=(...  60.8 us
    pallas_call x1, Pallas kernels, project(): pl.pallas_call(functools.partial(project_kernel, part), grid=(rows // blo...  14.6 us
    pallas_call x1, Pallas kernels, give_back(): pl.pallas_call(functools.partial(return_kernel, group, rows), out_shape=(...  14.3 us
    dot_general x1, matrix products, body(): jnp.dot(attended, out_proj, preferred_element_type=jnp.float32)  6.19 us
    pallas_call x1, Pallas kernels, swap(): pl.pallas_call(functools.partial(swap_kernel, n_tp), out_shape=jax.ShapeD...  4.48 us
    neg x1, other arithmetic, tables(): -sin_part  3.72 us

commit v1 on v0

v1 whole, which is shorter than its diff:
```python
import functools

import jax
import jax.numpy as jnp
from jax import lax
from jax.experimental import pallas as pl
from jax.experimental.pallas import tpu as pltpu
from jax.sharding import PartitionSpec as P

HEAD_DIM = 64
SPAN = 128
EPS = 1e-06
ROPE_BASE = 10000.0
WIDE = 16
LANES = 128
MESH = pl.DeviceIdType.MESH
ANY = pl.BlockSpec(memory_space=pl.ANY)
NEG = -1e30


def greet(peers):
    barrier = pltpu.get_barrier_semaphore()
    for peer in peers:
        pl.semaphore_signal(barrier, inc=1, device_id=peer, device_id_type=MESH)
    pl.semaphore_wait(barrier, len(peers))


def remote(src, dst, send, recv, peer):
    return pltpu.make_async_remote_copy(
        src_ref=src, dst_ref=dst, send_sem=send, recv_sem=recv, device_id=peer, device_id_type=MESH
    )


def group_of(mesh, width):
    for size in (4, 2):
        if mesh.shape["sp"] % size == 0 and width % (size * LANES) == 0:
            return size
    return 1


def flip(c, mask):
    out = c
    if mask & 1:
        out = out + 1 - 2 * lax.rem(c, 2)
    if mask & 2:
        out = out + 2 - 4 * lax.rem(lax.div(c, 2), 2)
    return out


def layer_kernel(
    n_sp, n_tp, group, behind,
    hid_ref, gain_ref, freq_ref, wq_ref, wk_ref, wv_ref,
    att_ref, lw_ref,
    hid, nrm, wq, wk, wv, cos_t, sin_t, scr,
    qn_all, kw_all, vw_all, qr_all, kx_all, vx_all,
    acc1, m1, l1, acc4, m4, l4, acc16, m16, l16, b1, b4, b16,
    local, near_s, near_r, line_s, line_r, dir_s, dir_r, across_s, across_r, twin_s, twin_r,
    early_s, early_r, late_s, late_r,
):
    f32, bf16 = jnp.float32, jnp.bfloat16
    s = lax.axis_index("sp")
    t = lax.axis_index("tp")
    rows, depth = hid_ref.shape
    all_rows = rows * group
    w_rows = wk_ref.shape[0]
    part = wq.shape[1]
    pairs = part // LANES
    steps = all_rows // WIDE
    few = rows // WIDE
    quarter = rows // 4
    count = n_sp // group
    c = lax.rem(s, group)
    base = s - c
    g = lax.div(s, group)
    half = lax.rem(t, 2)
    sibling = (s, t + 1 - 2 * half)
    masks = list(range(1, group))
    peer = {k: base + flip(c, k) for k in masks}
    up = lax.rem(s + group, n_sp)
    down = lax.rem(s + n_sp - group, n_sp)
    after = [lax.rem(s + b * group, n_sp) for b in range(1, behind + 1)]
    before = [lax.rem(s + n_sp - b * group, n_sp) for b in range(1, behind + 1)]
    start_row = pl.multiple_of(c * rows, rows)

    kept = [pltpu.make_async_copy(hid_ref, hid.at[pl.ds(start_row, rows)], local.at[0])]
    own_cols = pl.ds(pl.multiple_of(c * part, LANES), part)
    own_rows = pl.ds(pl.multiple_of(s * w_rows, w_rows), w_rows)
    kept.append(pltpu.make_async_copy(wq_ref.at[:, own_cols], wq, local.at[1]))
    for j, (src, dst) in enumerate(((wk_ref, wk), (wv_ref, wv))):
        kept.append(pltpu.make_async_copy(src.at[:, own_cols], dst.at[own_rows], local.at[2 + j]))
    for copy in kept:
        copy.start()

    known = [(peer[k], t) for k in masks] + [(x, t) for x in after + before] + [sibling]
    greet(known)

    def near(k, j):
        src, dst = ((wk_ref, wk), (wv_ref, wv))[j]
        cols = pl.ds(pl.multiple_of(flip(c, k) * part, LANES), part)
        return remote(src.at[:, cols], dst.at[own_rows], near_s.at[j, k - 1], near_r.at[j, k - 1], (peer[k], t))

    def line(way, j, d):
        ref = (wk, wv)[j]
        to, off = ((up, g - d), (down, g + d))[way]
        off = jnp.clip(off, 0, count - 1)
        slot = ref.at[pl.ds(pl.multiple_of(off * group * w_rows, group * w_rows), group * w_rows)]
        return remote(slot, slot, line_s.at[way, j, d], line_r.at[way, j, d + 1], (to, t))

    def line_in(way, j, d):
        ref = (wk, wv)[j]
        off = jnp.clip((g - d, g + d)[way], 0, count - 1)
        slot = ref.at[pl.ds(pl.multiple_of(off * group * w_rows, group * w_rows), group * w_rows)]
        return remote(slot, slot, line_s.at[way, j, d - 1], line_r.at[way, j, d], ((up, down)[way], t))

    def has_in(way, d):
        return g >= d if way == 0 else g + d < count

    def has_out(way, d):
        if way == 0:
            return (g >= d) & (g + 1 < count)
        return (g + d < count) & (g >= 1)

    def pass_on(j, d):
        for way in range(2):
            if not (isinstance(d, int) and d == 0):
                @pl.when(has_in(way, d))
                def _(way=way):
                    line_in(way, j, d).wait_recv()

            if not (isinstance(d, int) and d == count - 1):
                @pl.when(has_out(way, d))
                def _(way=way):
                    line(way, j, d).start()

    def passed(j, d):
        for way in range(2):
            @pl.when(has_out(way, d))
            def _(way=way):
                line(way, j, d).wait_send()

    def piece(block, side, q):
        return hid.at[pl.ds(pl.multiple_of(block * rows + side * (2 * quarter) + q * quarter, quarter), quarter)]

    def direct(k, q):
        src = hid_ref.at[pl.ds(pl.multiple_of(half * (2 * quarter) + q * quarter, quarter), quarter)]
        return remote(src, piece(c, half, q), dir_s.at[k - 1, q], dir_r.at[k - 1, q], (peer[k], t))

    def across(i):
        k, other = ((1, 2), (2, 1))[i]
        slot = piece(flip(c, k), half, i)
        return remote(slot, slot, across_s.at[i], across_r.at[i], (peer[other], t))

    def twin(k, q):
        slot = piece(flip(c, k), half, q)
        return remote(slot, slot, twin_s.at[k - 1, q], twin_r.at[k - 1, q], sibling)

    for j in range(2):
        for k in masks:
            near(k, j).start()
    firsts = {4: [(1, 0), (2, 1)], 2: [(1, 0)], 1: []}[group]
    seconds = {4: [(1, 1), (2, 0)], 2: [(1, 1)], 1: []}[group]
    thirds = {4: [(3, 0), (3, 1)], 2: [], 1: []}[group]
    for k, q in firsts + seconds:
        direct(k, q).start()

    def block_of(k):
        return flip(c, k) * rows

    def norm(k):
        def body(i, _):
            at = pl.ds(pl.multiple_of(block_of(k) + i * quarter, quarter), quarter)
            x = hid[at, :].astype(f32)
            scale = lax.rsqrt(jnp.mean(x * x, axis=-1, keepdims=True) + EPS)
            nrm[at, :] = (x * scale * gain_ref[...]).astype(bf16)
            return 0

        lax.fori_loop(0, 4, body, 0)

    front = lax.rem(lax.broadcasted_iota(jnp.int32, (rows, LANES), 1), HEAD_DIM) < HEAD_DIM // 2

    def project(k, j):
        row = pl.multiple_of(block_of(k), rows)
        here = pl.ds(row, rows)
        out = jnp.dot(nrm[here, :], (wq, wk, wv)[j][...], preferred_element_type=f32)
        nat = (qn_all, kw_all, vw_all)[j]
        res = (qr_all, kx_all, vx_all)[j]
        skip = 0 if j == 0 else SPAN
        skip_res = 0 if j == 0 else behind * steps
        step = pl.multiple_of(lax.div(row, WIDE), few)
        for i in range(pairs):
            u = out[:, i * LANES:(i + 1) * LANES]
            if j < 2:
                swapped = jnp.where(
                    front,
                    pltpu.roll(u, LANES - HEAD_DIM // 2, 1),
                    pltpu.roll(u, HEAD_DIM // 2, 1),
                )
                u = u * cos_t[here, :] + swapped * sin_t[here, :]
            if j == 0:
                u = u * HEAD_DIM ** (-0.5)
            nat[i, pl.ds(row + skip, rows), :] = u.astype(bf16)
            scr[i] = u
        for i in range(pairs):
            for r in range(WIDE):
                res[i, r, pl.ds(step + skip_res, few), :] = scr[i, pl.ds(r, few, stride=WIDE), :].astype(bf16)

    for j in range(2):
        for k in masks:
            near(k, j).wait_recv()
        kept[2 + j].wait()
        pass_on(j, 0)

    half_dim = HEAD_DIM // 2
    lo = lax.broadcasted_iota(jnp.int32, (LANES, LANES), 0).astype(f32) * freq_ref[...]
    cos_lo, sin_lo = jnp.cos(lo), jnp.sin(lo)
    lane = lax.rem(lax.broadcasted_iota(jnp.int32, (1, LANES), 1), HEAD_DIM)
    sign = jnp.where(lane < half_dim, -1.0, 1.0)

    def fill(i, _):
        hi = (base * rows + i * LANES).astype(f32) * freq_ref[...]
        cos_hi, sin_hi = jnp.cos(hi), jnp.sin(hi)
        at = pl.ds(pl.multiple_of(i * LANES, LANES), LANES)
        cos_t[at, :] = cos_lo * cos_hi - sin_lo * sin_hi
        sin_t[at, :] = (sin_lo * cos_hi + cos_lo * sin_hi) * sign
        return 0

    lax.fori_loop(0, all_rows // LANES, fill, 0)

    @pl.when(g < behind)
    def _():
        for pair in range(pairs):
            for ref in (kw_all, vw_all):
                @pl.when(g < 1)
                def _(ref=ref, pair=pair):
                    ref[pair, pl.ds(0, SPAN), :] = jnp.zeros((SPAN, LANES), bf16)
            for ref in (kx_all, vx_all):
                for b in range(1, behind + 1):
                    @pl.when(g < b)
                    def _(ref=ref, pair=pair, b=b):
                        ref[pair, :, pl.ds((behind - b) * steps, steps), :] = jnp.zeros((WIDE, steps, LANES), bf16)

    kept[0].wait()
    norm(0)
    kept[1].wait()
    project(0, 0)

    for k, q in firsts:
        direct(k, q).wait_recv()
        if group == 4:
            across(k - 1).start()
        twin(k, q).start()
    if count > 1:
        for j in range(2):
            pass_on(j, 1)
    for k, q in seconds:
        direct(k, q).wait_recv()
        twin(k, q).start()
    if count > 2:
        for j in range(2):
            pass_on(j, 2)
    for k in masks[:2]:
        for q in range(2):
            twin(k, q).wait_recv()
        norm(k)
        project(k, 0)
    if group == 4:
        for k, q in thirds:
            across(q).wait_recv()
            twin(k, q).start()
    if count > 3:
        for d in range(3, min(count, 4)):
            pass_on(0, d)
            pass_on(1, d)
    if count > 4:
        def further(d, _):
            pass_on(0, d)
            pass_on(1, d)
            return 0

        lax.fori_loop(4, count, further, 0)

    def early(pair, j):
        ref = (kw_all, vw_all)[j]
        return remote(
            ref.at[pair, pl.ds(all_rows, SPAN)], ref.at[pair, pl.ds(0, SPAN)],
            early_s.at[pair, j], early_r.at[pair, j], (after[0], t),
        )

    def late(pair, j, k, b):
        ref = (kx_all, vx_all)[j]
        at = pl.multiple_of(flip(c, k) * few, few)
        return remote(
            ref.at[pair, :, pl.ds(behind * steps + at, few)],
            ref.at[pair, :, pl.ds((behind - b) * steps + at, few)],
            late_s.at[pair, j, b - 1, k], late_r.at[pair, j, b - 1, k], (after[b - 1], t),
        )

    everything = [0] + masks

    def send_late(pair, j, k):
        for b in range(1, behind + 1):
            @pl.when(g + b < count)
            def _(b=b):
                late(pair, j, k, b).start()

    def send_early(pair, j):
        @pl.when(g + 1 < count)
        def _():
            early(pair, j).start()

    for k in everything[:3]:
        project(k, 1)
        if k > 0:
            send_late(0, 0, k - 1)
    if group == 4:
        for q in range(2):
            twin(3, q).wait_recv()
        norm(3)
        project(3, 0)
        project(3, 1)
        send_late(0, 0, 2)
    for i, k in enumerate(everything):
        project(k, 2)
        if i == 0:
            send_late(0, 0, everything[-1])
            send_early(0, 0)
        else:
            send_late(0, 1, k - 1)

    def put_bias(ref, near_by, first_of):
        shape = ref.shape[1:]
        a = lax.broadcasted_iota(jnp.int32, shape, 0)
        b = lax.broadcasted_iota(jnp.int32, shape, 1)
        distance, place = near_by(a, b)
        band = (distance >= 0) & (distance <= SPAN)
        ref[0] = jnp.where(band & (place + first_of >= 0), 0.0, NEG).astype(f32)
        ref[1] = jnp.where(band, 0.0, NEG).astype(f32)

    def plain(a, b):
        return a + SPAN - b, b - SPAN

    def woven(a, b):
        return 4 * (a % 32 + 32 - b % 64) + a // 32 - b // 64, b % 64 - 32

    put_bias(b1, plain, g * all_rows)
    put_bias(b16, plain, g * steps)
    put_bias(b4, woven, g * steps)

    send_late(0, 1, everything[-1])
    send_early(0, 1)
    for pair in range(1, pairs):
        for j in range(2):
            for k in everything:
                send_late(pair, j, k)
            send_early(pair, j)

    block = min(SPAN, steps)
    skip16 = behind * steps - SPAN

    def tile(q, k, v, bias):
        n = q.shape[0]
        low = lax.broadcasted_iota(jnp.int32, (n, LANES), 1) < HEAD_DIM
        low_q = low.astype(f32).astype(bf16)
        both = jnp.concatenate([q * low_q, q * (1 - low_q)], axis=0)
        sc = lax.dot_general(both, k, (((1,), (1,)), ((), ())), preferred_element_type=f32)
        sc = sc + jnp.concatenate([bias, bias], axis=0)
        m = jnp.max(sc, axis=-1, keepdims=True)
        e = jnp.exp(sc - m).astype(bf16)
        o = jnp.dot(e, jnp.concatenate([v, jnp.ones_like(v)], axis=1), preferred_element_type=f32)
        wide_m = jnp.broadcast_to(m, (2 * n, LANES))
        return (
            jnp.where(low, o[:n, :LANES], o[n:, :LANES]),
            jnp.where(low, wide_m[:n], wide_m[n:]),
            jnp.where(low, o[:n, LANES:], o[n:, LANES:]),
        )

    blocks16 = steps // block
    blocks4 = steps // 32

    for p in range(pairs):
        qn, kw, vw, qr, kx, vx = (ref.at[p] for ref in (qn_all, kw_all, vw_all, qr_all, kx_all, vx_all))

        def step16(idx, _):
            r = idx // blocks16
            i = idx % blocks16
            at = pl.multiple_of(i * block, block)
            keys = pl.ds(at + skip16, block + SPAN)
            got = tile(qr[r, pl.ds(at, block), :], kx[r, keys, :], vx[r, keys, :], b16[jnp.minimum(i, 1)])
            for ref, value in zip((acc16, m16, l16), got):
                ref[pl.ds(r + WIDE * at, block, stride=WIDE), :] = value
            return 0

        def step4(r, i):
            at = i * 32
            low = at + behind * steps - 32
            if not isinstance(i, int):
                at = pl.multiple_of(at, 32)
                low = pl.multiple_of(low, 32)
            keys = pl.ds(low, 64)
            got = tile(
                jnp.concatenate([qr[r + 4 * j, pl.ds(at, 32), :] for j in range(4)], axis=0),
                jnp.concatenate([kx[r + 4 * j, keys, :] for j in range(4)], axis=0),
                jnp.concatenate([vx[r + 4 * j, keys, :] for j in range(4)], axis=0),
                b4[0 if isinstance(i, int) else 1],
            )
            for ref, value in zip((acc4, m4, l4), got):
                for j in range(4):
                    ref[pl.ds(r + 4 * j + WIDE * at, 32, stride=WIDE), :] = value[j * 32:(j + 1) * 32]
            return 0

        def step1(i, _):
            at = pl.multiple_of(i * SPAN, SPAN)
            here = pl.ds(at, SPAN)
            keys = pl.ds(at, 2 * SPAN)
            got = tile(qn[here, :], kw[keys, :], vw[keys, :], b1[jnp.minimum(i, 1)])
            for ref, value in zip((acc1, m1, l1), got):
                ref[here, :] = value
            return 0

        def merge(i, _):
            here = pl.ds(pl.multiple_of(i * SPAN, SPAN), SPAN)
            tops = (m1[here, :], m4[here, :], m16[here, :])
            top = jnp.maximum(tops[0], jnp.maximum(tops[1], tops[2]))
            e1, e4, e16 = (jnp.exp(x - top) for x in tops)
            total = l1[here, :] * e1 + l4[here, :] * e4 + l16[here, :] * e16
            mixed = acc1[here, :] * e1 + acc4[here, :] * e4 + acc16[here, :] * e16
            att_ref[here, pl.ds(p * LANES, LANES)] = (mixed / total).astype(att_ref.dtype)
            turned = jnp.transpose(top + jnp.log(total))
            lw_ref[p, 0:1, here] = turned[0:1]
            lw_ref[p, 1:2, here] = turned[HEAD_DIM:HEAD_DIM + 1]
            return 0

        if blocks4 > 1:
            lax.fori_loop(
                0, 4 * (blocks4 - 1),
                lambda idx, _: step4(idx // (blocks4 - 1), idx % (blocks4 - 1) + 1), 0, unroll=2,
            )
        lax.fori_loop(1, all_rows // SPAN, step1, 0, unroll=2)
        for j in range(2):
            @pl.when(g >= 1)
            def _(j=j):
                early(p, j).wait_recv()
        step1(0, 0)
        for j in range(2):
            for b in range(1, behind + 1):
                @pl.when(g >= b)
                def _(j=j, b=b):
                    for k in everything:
                        late(p, j, k, b).wait_recv()
        lax.fori_loop(0, 4, lambda r, _: step4(r, 0), 0, unroll=2)
        lax.fori_loop(0, WIDE * blocks16, step16, 0, unroll=2)
        lax.fori_loop(0, all_rows // SPAN, merge, 0, unroll=2)

    for j in range(2):
        for k in masks:
            near(k, j).wait_send()
        for d in range(min(count - 1, 4)):
            passed(j, d)
        if count > 5:
            lax.fori_loop(4, count - 1, lambda d, _, j=j: (passed(j, d), 0)[1], 0)
    for k, q in firsts + seconds:
        direct(k, q).wait_send()
        twin(k, q).wait_send()
    if group == 4:
        for i in range(2):
            across(i).wait_send()
            twin(3, i).wait_send()
    for pair in range(pairs):
        for j in range(2):
            @pl.when(g + 1 < count)
            def _(pair=pair, j=j):
                early(pair, j).wait_send()

            for b in range(1, behind + 1):
                @pl.when(g + b < count)
                def _(pair=pair, j=j, b=b):
                    for k in everything:
                        late(pair, j, k, b).wait_send()


def layer(mesh, group, behind, hidden, gain, freq, wq, wk, wv):
    n_sp = mesh.shape["sp"]
    rows, depth = hidden.shape
    w_rows, width = wk.shape
    part = width // group
    pairs = part // LANES
    all_rows = rows * group
    steps = all_rows // WIDE
    block = min(SPAN, steps)
    count = n_sp // group
    f32, bf16 = jnp.float32, jnp.bfloat16
    dma = pltpu.SemaphoreType.DMA
    state = pltpu.VMEM((all_rows, LANES), f32)
    weight = pltpu.VMEM((depth, part), bf16)
    table = pltpu.VMEM((all_rows, LANES), f32)
    full = pltpu.VMEM((all_rows, depth), bf16)
    ring = pltpu.VMEM((pairs, SPAN + all_rows, LANES), bf16)
    woven = pltpu.VMEM((pairs, WIDE, (behind + 1) * steps, LANES), bf16)
    vmem = pl.BlockSpec(memory_space=pltpu.VMEM)
    near = max(group - 1, 1)
    return pl.pallas_call(
        functools.partial(layer_kernel, n_sp, mesh.shape["tp"], group, behind),
        out_shape=(
            jax.ShapeDtypeStruct((all_rows, part), bf16),
            jax.ShapeDtypeStruct((pairs, 2, all_rows), f32),
        ),
        in_specs=[ANY, vmem, vmem, ANY, ANY, ANY],
        out_specs=(vmem, vmem),
        scratch_shapes=[
            full, full, weight, weight, weight, table, table,
            pltpu.VMEM((pairs, rows, LANES), f32),
            pltpu.VMEM((pairs, all_rows, LANES), bf16), ring, ring,
            pltpu.VMEM((pairs, WIDE, steps, LANES), bf16), woven, woven,
            state, state, state, state, state, state, state, state, state,
            pltpu.VMEM((2, SPAN, 2 * SPAN), f32),
            pltpu.VMEM((2, SPAN, 2 * SPAN), f32),
            pltpu.VMEM((2, block, block + SPAN), f32),
            dma((4,)), dma((2, near)), dma((2, near)), dma((2, 2, count)), dma((2, 2, count)),
            dma((2, 2)), dma((2, 2)), dma((2,)), dma((2,)), dma((3, 2)), dma((3, 2)),
            dma((pairs, 2)), dma((pairs, 2)),
            dma((pairs, 2, behind, group)), dma((pairs, 2, behind, group)),
        ],
        compiler_params=pltpu.CompilerParams(
            vmem_limit_bytes=62 * 1024 * 1024, collective_id=0, has_side_effects=True
        ),
        name="layer_core",
    )(hidden, gain, freq, wq, wk, wv)


def return_kernel(group, rows, att_ref, lw_ref, att_out, lw_out, send, recv, local):
    s = lax.axis_index("sp")
    t = lax.axis_index("tp")
    part = att_ref.shape[1]
    c = lax.rem(s, group)
    base = s - c
    peers = [lax.rem(c + k, group) for k in range(1, group)]
    if group > 1:
        greet([(base + peer, t) for peer in peers])
    cols = pl.ds(pl.multiple_of(c * part, LANES), part)

    def pieces(peer):
        span = pl.ds(pl.multiple_of(peer * rows, rows), rows)
        return ((att_ref.at[span], att_out.at[:, cols]), (lw_ref.at[:, :, span], lw_out.at[c]))

    copies = []
    for k, peer in enumerate(peers):
        for j, (src, dst) in enumerate(pieces(peer)):
            copies.append(remote(src, dst, send.at[2 * k + j], recv.at[2 * k + j], (base + peer, t)))
    for j, (src, dst) in enumerate(pieces(c)):
        copies.append(pltpu.make_async_copy(src, dst, local.at[j]))
    for copy in copies:
        copy.start()
    for copy in copies:
        copy.wait()


def give_back(mesh, group, att, lw):
    rows = att.shape[0] // group
    part = att.shape[1]
    pairs = part // LANES
    dma = pltpu.SemaphoreType.DMA
    return pl.pallas_call(
        functools.partial(return_kernel, group, rows),
        out_shape=(
            jax.ShapeDtypeStruct((rows, part * group), att.dtype),
            jax.ShapeDtypeStruct((group, pairs, 2, rows), lw.dtype),
        ),
        in_specs=[ANY] * 2,
        out_specs=(ANY,) * 2,
        scratch_shapes=[dma((2 * group,)), dma((2 * group,)), dma((2,))],
        compiler_params=pltpu.CompilerParams(
            collective_id=2 if group > 1 else None, has_side_effects=True
        ),
        name="give_back",
    )(att, lw)


def swap_kernel(n_tp, part_ref, out_ref, send, recv):
    s = lax.axis_index("sp")
    t = lax.axis_index("tp")
    peers = [lax.rem(t + k, n_tp) for k in range(1, n_tp)]
    greet([(s, peer) for peer in peers])
    copies = [
        remote(part_ref.at[peer], out_ref.at[k], send.at[k], recv.at[k], (s, peer))
        for k, peer in enumerate(peers)
    ]
    for copy in copies:
        copy.start()
    for copy in copies:
        copy.wait()


def swap(mesh, partial):
    n_tp = mesh.shape["tp"]
    dma = pltpu.SemaphoreType.DMA
    return pl.pallas_call(
        functools.partial(swap_kernel, n_tp),
        out_shape=jax.ShapeDtypeStruct((n_tp - 1,) + partial.shape[1:], partial.dtype),
        in_specs=[ANY],
        out_specs=ANY,
        scratch_shapes=[dma((n_tp,)), dma((n_tp,))],
        compiler_params=pltpu.CompilerParams(collective_id=3, has_side_effects=True),
        name="swap_partials",
    )(partial)


def body(mesh, hidden_in, pre_gain, query_proj, key_proj, value_proj, out_proj, post_gain):
    rows, depth = hidden_in.shape
    width = query_proj.shape[1]
    n_tp = mesh.shape["tp"]
    group = group_of(mesh, width)
    t = lax.axis_index("tp")
    all_rows = rows * group
    behind = -(-(WIDE * SPAN) // all_rows)
    half_dim = HEAD_DIM // 2
    frequency = ROPE_BASE ** (-(jnp.arange(half_dim, dtype=jnp.float32) * 2.0 / HEAD_DIM))
    freq = jnp.concatenate([frequency] * (LANES // half_dim))[None, :]
    att, lw = layer(
        mesh, group, behind, hidden_in, pre_gain[None, :], freq, query_proj, key_proj, value_proj
    )
    attended, log_weight = give_back(mesh, group, att, lw)
    partial = jnp.dot(attended, out_proj, preferred_element_type=jnp.float32).astype(jnp.bfloat16)
    partial = partial.reshape(n_tp, rows // n_tp, depth)
    others = swap(mesh, partial)
    own = lax.dynamic_index_in_dim(partial, t, 0, keepdims=False)
    summed = own.astype(jnp.float32) + jnp.sum(others.astype(jnp.float32), axis=0)
    scale = lax.rsqrt(jnp.mean(summed * summed, axis=-1, keepdims=True) + EPS)
    layer_out = (summed * scale * post_gain).astype(jnp.bfloat16)
    return (layer_out, log_weight.reshape(width // HEAD_DIM, rows))


def solution(mesh):
    placed = (P("sp", None), P(), P(None, "tp"), P("sp", "tp"), P("sp", "tp"), P("tp", None), P())
    return jax.shard_map(
        functools.partial(body, mesh),
        mesh=mesh,
        in_specs=placed,
        out_specs=(P(("sp", "tp"), None), P("tp", "sp")),
        check_vma=False,
    )
```

time: 180 us -> 136 us (0.76); the launches traced: 177 us -> 136 us
  Pallas kernels: 155 us -> 124 us
  other arithmetic: 9.98 us -> 3.83 us
  local copies, waits for them, and re-layouts: 5.15 us -> 1.41 us
    pallas_call x3 -> x1, Pallas kernels: 136 us -> 105 us  [layer(): pl.pallas_call(functools.partial(layer_kernel, n_sp, mesh.shape['tp'], gr...]
    neg x1 -> x0, other arithmetic: 3.72 us -> none  [tables(): -sin_part]
    concatenate x1 -> x0, other arithmetic: 3.02 us -> none  [tables(): jnp.concatenate([cos_part] * 4, axis=1)]
    unnamed x12 -> x6, local copies, waits for them, and re-layouts: 2.46 us -> 0.01 us
where the time goes in v1:
time: 136 us
  Pallas kernels  124 us (91%)
  matrix products  6.19 us (5%)
  other arithmetic  3.83 us (3%)
  local copies, waits for them, and re-layouts  1.41 us (1%)
    pallas_call x1, Pallas kernels, layer(): pl.pallas_call(functools.partial(layer_kernel, n_sp, mesh.shape['tp'], gr...  105 us
    pallas_call x1, Pallas kernels, give_back(): pl.pallas_call(functools.partial(return_kernel, group, rows), out_shape=(...  15.9 us
    dot_general x1, matrix products, body(): jnp.dot(attended, out_proj, preferred_element_type=jnp.float32)  6.19 us
    pallas_call x1, Pallas kernels, swap(): pl.pallas_call(functools.partial(swap_kernel, n_tp), out_shape=jax.ShapeD...  3.16 us

profile of v1, /device:TPU:9, one launch (start us, length us, event | category | flops | bytes accessed | tf_op | source)
XLA Modules:
  0.0 135.8 jit_solution(11199667504436178003)
XLA Ops:
  0.6 0.6 maximum_bitcast_fusion.freq_ref
  1.2 104.6 %layer_core.1 = (bf16[2048,256]{1,0:T(8,128)(2,1)}, f32[2,2,2048]{2,1,0:T(2,128)}) custom-call(bf16[512,2048]{1,0:T(8,128)(2,1)} %hid_ref.1, f32[1,2048]{1,0:T(1,128)} %bitcast.18, f32[1,128]{1,0:T(1,128)} %maximum_bitcast_fusion.freq_ref, bf16[2048,1024]{1,0:T(8,128)(2,1)} %wq_ref.1, bf16[128,1024]{1,0:T(8,128)(2,1)} %wk_ref.1, bf16[128,1024]{1,0:T(8,128)(2,1)} %wv_ref.1), custom_call_target="tpu_custom_call" | custom-call | tf_op jit(solution)/shard_map/layer_core/pallas_call | solution.py:501
  105.8 15.9 %give_back.1 = (bf16[512,1024]{1,0:T(8,128)(2,1)}, f32[4,2,2,512]{3,2,1,0:T(2,128)}) custom-call(bf16[2048,256]{1,0:T(8,128)(2,1)} %get-tuple-element.6.att_ref, f32[2,2,2048]{2,1,0:T(2,128)} %get-tuple-element.7.lw_ref), custom_call_target="tpu_custom_call" | custom-call | tf_op jit(solution)/shard_map/give_back/pallas_call | solution.py:562
  121.7 1.4 %reshape.23 = f32[16,512]{1,0:T(8,128)} reshape(f32[4,2,2,512]{3,2,1,0:T(2,128)} %get-tuple-element.9) | data formatting | bytes 65536 | tf_op jit(solution)/shard_map/reshape | solution.py:629
  123.1 6.2 %convolution_convert_fusion = bf16[512,2048]{1,0:T(8,128)(2,1)} fusion(bf16[512,1024]{1,0:T(8,128)(2,1)} %get-tuple-element.8, bf16[1024,2048]{1,0:T(8,128)(2,1)} %param.12), kind=kOutput, calls=%fused_computation | convolution fusion | flops 2148532224 | bytes 7340032 | tf_op jit(solution)/shard_map/dot_general | solution.py:622
  129.3 0.0 copy-start.1
  129.3 0.0 copy-start.2
  129.3 3.2 %swap_partials.1 = bf16[1,256,2048]{2,1,0:T(8,128)(2,1)} custom-call(bf16[2,256,2048]{2,1,0:T(8,128)(2,1)} %bitcast.15), custom_call_target="tpu_custom_call" | custom-call | tf_op jit(solution)/shard_map/swap_partials/pallas_call | solution.py:596
  132.5 0.0 copy-done.1
  132.5 0.0 copy-start
  132.5 1.7 %fusion = f32[256]{0:T(256)S(1)} fusion(bf16[1,256,2048]{2,1,0:T(8,128)(2,1)} %swap_partials.1, bf16[2,256,2048]{2,1,0:T(8,128)(2,1)S(1)} %bitcast.16, s32[]{:T(128)S(6)} %select_n.4), kind=kLoop, calls=%fused_computation.3 | loop fusion | flops 2621184 | bytes 2098180 | tf_op jit(solution)/shard_map/reduce_sum | solution.py:627
  134.3 0.0 copy-done.2
  134.3 0.0 copy-done
  134.3 1.5 %fusion.2 = bf16[256,2048]{1,0:T(8,128)(2,1)} fusion(bf16[1,256,2048]{2,1,0:T(8,128)(2,1)S(1)} %copy-done, f32[2048]{0:T(1024)S(1)} %copy-done.2, f32[256]{0:T(256)S(1)} %add_rsqrt_fusion, bf16[2,256,2048]{2,1,0:T(8,128)(2,1)S(1)} %bitcast.17, s32[]{:T(128)S(6)} %select_n.4), kind=kLoop, calls=%fused_computation.5 | loop fusion | flops 3145728 | bytes 3154948 | tf_op jit(solution)/shard_map/convert_element_type | solution.py:628
  (2 shorter events, 0.0 us)
Async XLA Ops:
  129.3 3.2 %copy-start.1 = (bf16[512,2048]{1,0:T(8,128)(2,1)S(1)}, bf16[512,2048]{1,0:T(8,128)(2,1)}, u32[]{:S(2)}) copy-start(bf16[512,2048]{1,0:T(8,128)(2,1)} %convolution_convert_fusion) | copy-start | bytes 6291460
  129.3 4.9 %copy-start.2 = (f32[2048]{0:T(1024)S(1)}, f32[2048]{0:T(1024)}, u32[]{:S(2)}) copy-start(f32[2048]{0:T(1024)} %param.13) | copy-start | bytes 24580
  132.5 1.8 %copy-start = (bf16[1,256,2048]{2,1,0:T(8,128)(2,1)S(1)}, bf16[1,256,2048]{2,1,0:T(8,128)(2,1)}, u32[]{:S(2)}) copy-start(bf16[1,256,2048]{2,1,0:T(8,128)(2,1)} %swap_partials.1) | copy-start | bytes 3145732

commit v2 on v1

v2 whole, which is shorter than its diff:
```python
import functools

import jax
import jax.numpy as jnp
from jax import lax
from jax.experimental import pallas as pl
from jax.experimental.pallas import tpu as pltpu
from jax.sharding import PartitionSpec as P

HEAD_DIM = 64
SPAN = 128
EPS = 1e-06
ROPE_BASE = 10000.0
WIDE = 16
LANES = 128
MESH = pl.DeviceIdType.MESH
ANY = pl.BlockSpec(memory_space=pl.ANY)
NEG = -1e30


def remote(src, dst, send, recv, peer):
    return pltpu.make_async_remote_copy(
        src_ref=src, dst_ref=dst, send_sem=send, recv_sem=recv, device_id=peer, device_id_type=MESH
    )


def group_of(mesh, width):
    for size in (4, 2):
        if mesh.shape["sp"] % size == 0 and width % (size * LANES) == 0:
            return size
    return 1


def flip(c, mask):
    out = c
    if mask & 1:
        out = out + 1 - 2 * lax.rem(c, 2)
    if mask & 2:
        out = out + 2 - 4 * lax.rem(lax.div(c, 2), 2)
    return out


def layer_kernel(
    n_sp, n_tp, group, behind,
    hid_ref, gain_ref, freq_ref, wq_ref, wk_ref, wv_ref, wo_ref, post_ref,
    out_ref, lw_ref,
    raw, nrm, wq, wk, wv, wo, cos_t, sin_t, scr,
    qn_all, kw_all, vw_all, qr_all, kx_all, vx_all,
    acc1, m1, l1, acc4, m4, l4, acc16, m16, l16, b1, b4, b16,
    att, att_in, lw, lw_in, total, snd, rcv,
    local, near_s, near_r, line_s, line_r, dir_s, dir_r, across_s, across_r, twin_s, twin_r,
    early_s, early_r, late_s, late_r, back_s, back_r, swap_s, swap_r,
):
    f32, bf16 = jnp.float32, jnp.bfloat16
    s = lax.axis_index("sp")
    t = lax.axis_index("tp")
    rows, depth = hid_ref.shape
    all_rows = rows * group
    w_rows = wk_ref.shape[0]
    part = wq.shape[1]
    pairs = part // LANES
    steps = all_rows // WIDE
    few = rows // WIDE
    quarter = rows // 4
    count = n_sp // group
    c = lax.rem(s, group)
    base = s - c
    g = lax.div(s, group)
    half = lax.rem(t, 2)
    sibling = (s, t + 1 - 2 * half)
    masks = list(range(1, group))
    peer = {k: base + flip(c, k) for k in masks}
    up = lax.rem(s + group, n_sp)
    down = lax.rem(s + n_sp - group, n_sp)
    after = [lax.rem(s + b * group, n_sp) for b in range(1, behind + 1)]
    before = [lax.rem(s + n_sp - b * group, n_sp) for b in range(1, behind + 1)]
    start_row = pl.multiple_of(c * rows, rows)

    kept = [pltpu.make_async_copy(hid_ref, raw, local.at[0])]
    own_cols = pl.ds(pl.multiple_of(c * part, LANES), part)
    own_rows = pl.ds(pl.multiple_of(s * w_rows, w_rows), w_rows)
    kept.append(pltpu.make_async_copy(wq_ref.at[:, own_cols], wq, local.at[1]))
    for j, (src, dst) in enumerate(((wk_ref, wk), (wv_ref, wv))):
        kept.append(pltpu.make_async_copy(src.at[:, own_cols], dst.at[own_rows], local.at[2 + j]))
    for p in range(pairs):
        for i in range(group):
            kept.append(pltpu.make_async_copy(
                wo_ref.at[pl.ds(i * part + p * LANES, LANES)], wo.at[p, pl.ds(i * LANES, LANES)],
                local.at[4 + p * group + i],
            ))
    for copy in kept:
        copy.start()

    known = [(peer[k], t) for k in masks] + [(x, t) for x in after + before]
    known += [(s, lax.rem(t + k, n_tp)) for k in range(1, n_tp)]
    barrier = pltpu.get_barrier_semaphore()
    for other in known:
        pl.semaphore_signal(barrier, inc=1, device_id=other, device_id_type=MESH)

    half_dim = HEAD_DIM // 2
    lo = lax.broadcasted_iota(jnp.int32, (LANES, LANES), 0).astype(f32) * freq_ref[...]
    cos_lo, sin_lo = jnp.cos(lo), jnp.sin(lo)
    lane = lax.rem(lax.broadcasted_iota(jnp.int32, (1, LANES), 1), HEAD_DIM)
    sign = jnp.where(lane < half_dim, -1.0, 1.0)

    def fill(i, _):
        hi = (base * rows + i * LANES).astype(f32) * freq_ref[...]
        cos_hi, sin_hi = jnp.cos(hi), jnp.sin(hi)
        at = pl.ds(pl.multiple_of(i * LANES, LANES), LANES)
        cos_t[at, :] = cos_lo * cos_hi - sin_lo * sin_hi
        sin_t[at, :] = (sin_lo * cos_hi + cos_lo * sin_hi) * sign
        return 0

    lax.fori_loop(0, all_rows // LANES, fill, 0)

    @pl.when(g < behind)
    def _():
        for pair in range(pairs):
            for ref in (kw_all, vw_all):
                @pl.when(g < 1)
                def _(ref=ref, pair=pair):
                    ref[pair, pl.ds(0, SPAN), :] = jnp.zeros((SPAN, LANES), bf16)
            for ref in (kx_all, vx_all):
                for b in range(1, behind + 1):
                    @pl.when(g < b)
                    def _(ref=ref, pair=pair, b=b):
                        ref[pair, :, pl.ds((behind - b) * steps, steps), :] = jnp.zeros((WIDE, steps, LANES), bf16)

    pl.semaphore_wait(barrier, len(known))

    def near(k, j):
        src, dst = ((wk_ref, wk), (wv_ref, wv))[j]
        cols = pl.ds(pl.multiple_of(flip(c, k) * part, LANES), part)
        return remote(src.at[:, cols], dst.at[own_rows], near_s.at[j, k - 1], near_r.at[j, k - 1], (peer[k], t))

    def line(way, j, d):
        ref = (wk, wv)[j]
        to, off = ((up, g - d), (down, g + d))[way]
        off = jnp.clip(off, 0, count - 1)
        slot = ref.at[pl.ds(pl.multiple_of(off * group * w_rows, group * w_rows), group * w_rows)]
        return remote(slot, slot, line_s.at[way, j, d], line_r.at[way, j, d + 1], (to, t))

    def line_in(way, j, d):
        ref = (wk, wv)[j]
        off = jnp.clip((g - d, g + d)[way], 0, count - 1)
        slot = ref.at[pl.ds(pl.multiple_of(off * group * w_rows, group * w_rows), group * w_rows)]
        return remote(slot, slot, line_s.at[way, j, d - 1], line_r.at[way, j, d], ((up, down)[way], t))

    def has_in(way, d):
        return g >= d if way == 0 else g + d < count

    def has_out(way, d):
        if way == 0:
            return (g >= d) & (g + 1 < count)
        return (g + d < count) & (g >= 1)

    def pass_on(j, d):
        for way in range(2):
            if not (isinstance(d, int) and d == 0):
                @pl.when(has_in(way, d))
                def _(way=way):
                    line_in(way, j, d).wait_recv()

            if not (isinstance(d, int) and d == count - 1):
                @pl.when(has_out(way, d))
                def _(way=way):
                    line(way, j, d).start()

    def passed(j, d):
        for way in range(2):
            @pl.when(has_out(way, d))
            def _(way=way):
                line(way, j, d).wait_send()

    def piece(block, side, q):
        return nrm.at[pl.ds(pl.multiple_of(block * rows + side * (2 * quarter) + q * quarter, quarter), quarter)]

    def direct(k, q):
        slot = piece(c, half, q)
        return remote(slot, slot, dir_s.at[k - 1, q], dir_r.at[k - 1, q], (peer[k], t))

    def across(i):
        k, other = ((1, 2), (2, 1))[i]
        slot = piece(flip(c, k), half, i)
        return remote(slot, slot, across_s.at[i], across_r.at[i], (peer[other], t))

    def twin(k, q):
        slot = piece(flip(c, k), half, q)
        return remote(slot, slot, twin_s.at[k - 1, q], twin_r.at[k - 1, q], sibling)

    for j in range(2):
        for k in masks:
            near(k, j).start()
    firsts = {4: [(1, 0), (2, 1)], 2: [(1, 0)], 1: []}[group]
    seconds = {4: [(1, 1), (2, 0)], 2: [(1, 1)], 1: []}[group]
    thirds = {4: [(3, 0), (3, 1)], 2: [], 1: []}[group]
    def block_of(k):
        return flip(c, k) * rows

    kept[0].wait()

    def norm(i, _):
        x = raw[pl.ds(pl.multiple_of(i * quarter, quarter), quarter), :].astype(f32)
        scale = lax.rsqrt(jnp.mean(x * x, axis=-1, keepdims=True) + EPS)
        at = pl.ds(pl.multiple_of(start_row + i * quarter, quarter), quarter)
        nrm[at, :] = (x * scale * gain_ref[...]).astype(bf16)
        return 0

    lax.fori_loop(0, 4, norm, 0)

    def put_bias(ref, near_by, first_of):
        shape = ref.shape[1:]
        a = lax.broadcasted_iota(jnp.int32, shape, 0)
        b = lax.broadcasted_iota(jnp.int32, shape, 1)
        distance, place = near_by(a, b)
        band = (distance >= 0) & (distance <= SPAN)
        ref[0] = jnp.where(band & (place + first_of >= 0), 0.0, NEG).astype(f32)
        ref[1] = jnp.where(band, 0.0, NEG).astype(f32)

    def plain(a, b):
        return a + SPAN - b, b - SPAN

    def woven(a, b):
        return 4 * (a % 32 + 32 - b % 64) + a // 32 - b // 64, b % 64 - 32

    put_bias(b1, plain, g * all_rows)
    put_bias(b16, plain, g * steps)
    put_bias(b4, woven, g * steps)

    for k, q in firsts + seconds:
        direct(k, q).start()

    front = lax.rem(lax.broadcasted_iota(jnp.int32, (rows, LANES), 1), HEAD_DIM) < HEAD_DIM // 2

    def project(k, j):
        row = pl.multiple_of(block_of(k), rows)
        here = pl.ds(row, rows)
        out = jnp.dot(nrm[here, :], (wq, wk, wv)[j][...], preferred_element_type=f32)
        nat = (qn_all, kw_all, vw_all)[j]
        res = (qr_all, kx_all, vx_all)[j]
        skip = 0 if j == 0 else SPAN
        skip_res = 0 if j == 0 else behind * steps
        step = pl.multiple_of(lax.div(row, WIDE), few)
        for i in range(pairs):
            u = out[:, i * LANES:(i + 1) * LANES]
            if j < 2:
                swapped = jnp.where(
                    front,
                    pltpu.roll(u, LANES - HEAD_DIM // 2, 1),
                    pltpu.roll(u, HEAD_DIM // 2, 1),
                )
                u = u * cos_t[here, :] + swapped * sin_t[here, :]
            if j == 0:
                u = u * HEAD_DIM ** (-0.5)
            nat[i, pl.ds(row + skip, rows), :] = u.astype(bf16)
            scr[i] = u
        for i in range(pairs):
            for r in range(WIDE):
                res[i, 4 * (r % 4) + r // 4, pl.ds(step + skip_res, few), :] = scr[i, pl.ds(r, few, stride=WIDE), :].astype(bf16)

    for j in range(2):
        for k in masks:
            near(k, j).wait_recv()
        kept[2 + j].wait()
        pass_on(j, 0)

    kept[1].wait()
    project(0, 0)

    for k, q in firsts:
        direct(k, q).wait_recv()
        if group == 4:
            across(k - 1).start()
        twin(k, q).start()
    if count > 1:
        for j in range(2):
            pass_on(j, 1)
    for k, q in seconds:
        direct(k, q).wait_recv()
        twin(k, q).start()
    if count > 2:
        for j in range(2):
            pass_on(j, 2)
    for k in masks[:2]:
        for q in range(2):
            twin(k, q).wait_recv()
        project(k, 0)

    def far(j):
        if count > 3:
            pass_on(j, 3)
        if count > 4:
            lax.fori_loop(4, count, lambda d, _: (pass_on(j, d), 0)[1], 0)

    def early(pair, j):
        ref = (kw_all, vw_all)[j]
        return remote(
            ref.at[pair, pl.ds(all_rows, SPAN)], ref.at[pair, pl.ds(0, SPAN)],
            early_s.at[pair, j], early_r.at[pair, j], (after[0], t),
        )

    def late(pair, j, k, b):
        ref = (kx_all, vx_all)[j]
        at = pl.multiple_of(flip(c, k) * few, few)
        return remote(
            ref.at[pair, :, pl.ds(behind * steps + at, few)],
            ref.at[pair, :, pl.ds((behind - b) * steps + at, few)],
            late_s.at[pair, j, b - 1, k], late_r.at[pair, j, b - 1, k], (after[b - 1], t),
        )

    everything = [0] + masks

    def send_late(pair, j, k):
        for b in range(1, behind + 1):
            @pl.when(g + b < count)
            def _(b=b):
                late(pair, j, k, b).start()

    def send_early(pair, j):
        @pl.when(g + 1 < count)
        def _():
            early(pair, j).start()

    for j in range(2):
        far(j)
        for i, k in enumerate(everything[:3]):
            project(k, 1 + j)
            if i > 0:
                send_late(0, j, k - 1)
            elif j == 1:
                send_late(0, 0, everything[:3][-1])
    if group == 4:
        for k, q in thirds:
            across(q).wait_recv()
            twin(k, q).start()
        send_late(0, 1, 2)
        for q in range(2):
            twin(3, q).wait_recv()
        project(3, 1)
        project(3, 2)
        send_late(0, 0, 3)
        project(3, 0)
        send_late(0, 1, 3)
    else:
        send_late(0, 1, everything[-1])
    for j in range(2):
        send_early(0, j)

    def part_of(pair, j, u, b):
        ref = (kx_all, vx_all)[j]
        return remote(
            ref.at[pair, pl.ds(4 * u, 4), pl.ds(behind * steps, steps)],
            ref.at[pair, pl.ds(4 * u, 4), pl.ds((behind - b) * steps, steps)],
            late_s.at[pair, j, b - 1, u], late_r.at[pair, j, b - 1, u], (after[b - 1], t),
        )

    for pair in range(1, pairs):
        for j in range(2):
            send_early(pair, j)
        for u in range(4):
            for j in range(2):
                for b in range(1, behind + 1):
                    @pl.when(g + b < count)
                    def _(pair=pair, j=j, u=u, b=b):
                        part_of(pair, j, u, b).start()

    block = min(SPAN, steps)
    skip16 = behind * steps - SPAN

    def tile(q, k, v, bias):
        n = q.shape[0]
        low = lax.broadcasted_iota(jnp.int32, (n, LANES), 1) < HEAD_DIM
        low_q = low.astype(f32).astype(bf16)
        both = jnp.concatenate([q * low_q, q * (1 - low_q)], axis=0)
        sc = lax.dot_general(both, k, (((1,), (1,)), ((), ())), preferred_element_type=f32)
        sc = sc + jnp.concatenate([bias, bias], axis=0)
        m = jnp.max(sc, axis=-1, keepdims=True)
        e = jnp.exp(sc - m).astype(bf16)
        o = jnp.dot(e, jnp.concatenate([v, jnp.ones_like(v)], axis=1), preferred_element_type=f32)
        wide_m = jnp.broadcast_to(m, (2 * n, LANES))
        return (
            jnp.where(low, o[:n, :LANES], o[n:, :LANES]),
            jnp.where(low, wide_m[:n], wide_m[n:]),
            jnp.where(low, o[:n, LANES:], o[n:, LANES:]),
        )

    blocks16 = steps // block
    blocks4 = steps // 32

    def back(p, k):
        to = (peer[k], t)
        span = pl.ds(pl.multiple_of(flip(c, k) * rows, rows), rows)
        mine = pl.ds(pl.multiple_of(c * LANES, LANES), LANES)
        return (
            remote(att.at[p, span], att_in.at[p, :, mine], back_s.at[p, k - 1, 0], back_r.at[p, k - 1, 0], to),
            remote(lw.at[p, :, span], lw_in.at[c, p], back_s.at[p, k - 1, 1], back_r.at[p, k - 1, 1], to),
        )

    def mix_out(p):
        for copy in kept[4 + p * group:4 + (p + 1) * group]:
            copy.wait()
        for k in masks:
            for copy in back(p, k):
                copy.wait_recv()
        value = jnp.dot(att_in[p], wo[p], preferred_element_type=f32)
        total[...] = value if p == 0 else total[...] + value

    for p in range(pairs):
        qn, kw, vw, qr, kx, vx = (ref.at[p] for ref in (qn_all, kw_all, vw_all, qr_all, kx_all, vx_all))

        def step16(idx, _):
            slot = idx // blocks16
            i = idx % blocks16
            r = 4 * (slot % 4) + slot // 4
            at = pl.multiple_of(i * block, block)
            keys = pl.ds(at + skip16, block + SPAN)
            got = tile(
                qr[slot, pl.ds(at, block), :], kx[slot, keys, :], vx[slot, keys, :], b16[jnp.minimum(i, 1)]
            )
            for ref, value in zip((acc16, m16, l16), got):
                ref[pl.ds(r + WIDE * at, block, stride=WIDE), :] = value
            return 0

        def step4(r, i):
            at = i * 32
            low = at + behind * steps - 32
            if not isinstance(i, int):
                at = pl.multiple_of(at, 32)
                low = pl.multiple_of(low, 32)
            keys = pl.ds(low, 64)
            got = tile(
                jnp.concatenate([qr[4 * r + j, pl.ds(at, 32), :] for j in range(4)], axis=0),
                jnp.concatenate([kx[4 * r + j, keys, :] for j in range(4)], axis=0),
                jnp.concatenate([vx[4 * r + j, keys, :] for j in range(4)], axis=0),
                b4[0 if isinstance(i, int) else 1],
            )
            for ref, value in zip((acc4, m4, l4), got):
                for j in range(4):
                    ref[pl.ds(r + 4 * j + WIDE * at, 32, stride=WIDE), :] = value[j * 32:(j + 1) * 32]
            return 0

        def step1(i, _):
            at = pl.multiple_of(i * SPAN, SPAN)
            here = pl.ds(at, SPAN)
            keys = pl.ds(at, 2 * SPAN)
            got = tile(qn[here, :], kw[keys, :], vw[keys, :], b1[jnp.minimum(i, 1)])
            for ref, value in zip((acc1, m1, l1), got):
                ref[here, :] = value
            return 0

        def merge(i, _):
            here = pl.ds(pl.multiple_of(i * SPAN, SPAN), SPAN)
            tops = (m1[here, :], m4[here, :], m16[here, :])
            top = jnp.maximum(tops[0], jnp.maximum(tops[1], tops[2]))
            e1, e4, e16 = (jnp.exp(x - top) for x in tops)
            whole = l1[here, :] * e1 + l4[here, :] * e4 + l16[here, :] * e16
            mixed = acc1[here, :] * e1 + acc4[here, :] * e4 + acc16[here, :] * e16
            att[p, here, :] = (mixed / whole).astype(bf16)
            turned = jnp.transpose(top + jnp.log(whole))
            lw[p, 0:1, here] = turned[0:1]
            lw[p, 1:2, here] = turned[HEAD_DIM:HEAD_DIM + 1]
            return 0

        if blocks4 > 1:
            lax.fori_loop(
                0, 4 * (blocks4 - 1),
                lambda idx, _: step4(idx // (blocks4 - 1), idx % (blocks4 - 1) + 1), 0, unroll=2,
            )
        lax.fori_loop(1, all_rows // SPAN, step1, 0, unroll=2)
        for j in range(2):
            @pl.when(g >= 1)
            def _(j=j):
                early(p, j).wait_recv()
        step1(0, 0)
        if p > 0:
            mix_out(p - 1)
        if p == 0:
            for j in range(2):
                for b in range(1, behind + 1):
                    @pl.when(g >= b)
                    def _(j=j, b=b):
                        for k in everything:
                            late(0, j, k, b).wait_recv()
            lax.fori_loop(0, 4, lambda r, _: step4(r, 0), 0, unroll=2)
            lax.fori_loop(0, WIDE * blocks16, step16, 0, unroll=2)
        else:
            def chunk(u, _):
                for j in range(2):
                    for b in range(1, behind + 1):
                        @pl.when(g >= b)
                        def _(j=j, b=b):
                            part_of(p, j, u, b).wait_recv()
                step4(u, 0)
                lax.fori_loop(0, 4 * blocks16, lambda n, _: step16(4 * blocks16 * u + n, 0), 0, unroll=2)
                return 0

            lax.fori_loop(0, 4, chunk, 0)
        order = masks[::-1] + [0]
        tiles = rows // SPAN
        for i, k in enumerate(order):
            first = flip(c, k) * tiles
            lax.fori_loop(0, tiles, lambda n, _: merge(first + n, 0), 0, unroll=2)
            if i > 0:
                for copy in back(p, order[i - 1]):
                    copy.start()
        here = pl.ds(start_row, rows)
        mine = pl.ds(pl.multiple_of(c * LANES, LANES), LANES)
        att_in[p, :, mine] = att[p, here, :]
        lw_in[c, p] = lw[p, :, here]

    last = pairs - 1
    for copy in kept[4 + last * group:]:
        copy.wait()
    for k in masks:
        for copy in back(last, k):
            copy.wait_recv()
    share = rows // n_tp
    sub = share // 2

    def finish(owner, i):
        here = pl.ds(pl.multiple_of(owner * share + i * sub, sub), sub)
        value = jnp.dot(att_in[last, here, :], wo[last], preferred_element_type=f32)
        if last > 0:
            value = value + total[here, :]
        return value.astype(bf16)

    def swap(k, i):
        at = pl.ds(i * sub, sub)
        return remote(
            snd.at[k - 1, at], rcv.at[k - 1, at], swap_s.at[k - 1, i], swap_r.at[k - 1, i],
            (s, lax.rem(t + k, n_tp)),
        )

    waiting = []
    for k in range(1, n_tp):
        for i in range(2):
            snd[k - 1, pl.ds(i * sub, sub), :] = finish(lax.rem(t + k, n_tp), i)
            if waiting:
                waiting.pop().start()
            waiting.append(swap(k, i))
    for i in range(2):
        at = pl.ds(i * sub, sub)
        total[at, :] = finish(t, i).astype(f32)
        if waiting:
            waiting.pop().start()
    heads = 2 * pairs
    for i in range(group):
        for p in range(pairs):
            for h in range(2):
                row = i * heads + p * 2 + h
                lw_ref[row:row + 1, :] = lw_in[i, p, h:h + 1, :]
    for i in range(2):
        at = pl.ds(i * sub, sub)
        value = total[at, :]
        for k in range(1, n_tp):
            swap(k, i).wait_recv()
            value = value + rcv[k - 1, at, :].astype(f32)
        scale = lax.rsqrt(jnp.mean(value * value, axis=-1, keepdims=True) + EPS)
        out_ref[at, :] = (value * scale * post_ref[...]).astype(bf16)

    for k in range(1, n_tp):
        for i in range(2):
            swap(k, i).wait_send()
    for p in range(pairs):
        for k in masks:
            for copy in back(p, k):
                copy.wait_send()
    for j in range(2):
        for k in masks:
            near(k, j).wait_send()
        for d in range(min(count - 1, 4)):
            passed(j, d)
        if count > 5:
            lax.fori_loop(4, count - 1, lambda d, _, j=j: (passed(j, d), 0)[1], 0)
    for k, q in firsts + seconds:
        direct(k, q).wait_send()
        twin(k, q).wait_send()
    if group == 4:
        for i in range(2):
            across(i).wait_send()
            twin(3, i).wait_send()
    for pair in range(pairs):
        for j in range(2):
            @pl.when(g + 1 < count)
            def _(pair=pair, j=j):
                early(pair, j).wait_send()

            for b in range(1, behind + 1):
                @pl.when(g + b < count)
                def _(pair=pair, j=j, b=b):
                    if pair == 0:
                        for k in everything:
                            late(pair, j, k, b).wait_send()
                    else:
                        for u in range(4):
                            part_of(pair, j, u, b).wait_send()


def layer(mesh, group, behind, hidden, gain, freq, wq, wk, wv, wo, post):
    n_sp = mesh.shape["sp"]
    n_tp = mesh.shape["tp"]
    rows, depth = hidden.shape
    w_rows, width = wk.shape
    part = width // group
    pairs = part // LANES
    all_rows = rows * group
    steps = all_rows // WIDE
    block = min(SPAN, steps)
    count = n_sp // group
    share = rows // n_tp
    f32, bf16 = jnp.float32, jnp.bfloat16
    dma = pltpu.SemaphoreType.DMA
    state = pltpu.VMEM((all_rows, LANES), f32)
    weight = pltpu.VMEM((depth, part), bf16)
    table = pltpu.VMEM((all_rows, LANES), f32)
    ring = pltpu.VMEM((pairs, SPAN + all_rows, LANES), bf16)
    woven = pltpu.VMEM((pairs, WIDE, (behind + 1) * steps, LANES), bf16)
    pieces = pltpu.VMEM((n_tp - 1, share, depth), bf16)
    vmem = pl.BlockSpec(memory_space=pltpu.VMEM)
    near = max(group - 1, 1)
    return pl.pallas_call(
        functools.partial(layer_kernel, n_sp, n_tp, group, behind),
        out_shape=(
            jax.ShapeDtypeStruct((share, depth), bf16),
            jax.ShapeDtypeStruct((width // HEAD_DIM, rows), f32),
        ),
        in_specs=[ANY, vmem, vmem, ANY, ANY, ANY, ANY, vmem],
        out_specs=(vmem, vmem),
        scratch_shapes=[
            pltpu.VMEM((rows, depth), bf16), pltpu.VMEM((all_rows, depth), bf16),
            weight, weight, weight, pltpu.VMEM((pairs, group * LANES, depth), bf16), table, table,
            pltpu.VMEM((pairs, rows, LANES), f32),
            pltpu.VMEM((pairs, all_rows, LANES), bf16), ring, ring,
            pltpu.VMEM((pairs, WIDE, steps, LANES), bf16), woven, woven,
            state, state, state, state, state, state, state, state, state,
            pltpu.VMEM((2, SPAN, 2 * SPAN), f32),
            pltpu.VMEM((2, SPAN, 2 * SPAN), f32),
            pltpu.VMEM((2, block, block + SPAN), f32),
            pltpu.VMEM((pairs, all_rows, LANES), bf16), pltpu.VMEM((pairs, rows, group * LANES), bf16),
            pltpu.VMEM((pairs, 2, all_rows), f32), pltpu.VMEM((group, pairs, 2, rows), f32),
            pltpu.VMEM((rows, depth), f32), pieces, pieces,
            dma((4 + pairs * group,)),
            dma((2, near)), dma((2, near)), dma((2, 2, count)), dma((2, 2, count)),
            dma((2, 2)), dma((2, 2)), dma((2,)), dma((2,)), dma((3, 2)), dma((3, 2)),
            dma((pairs, 2)), dma((pairs, 2)),
            dma((pairs, 2, behind, 4)), dma((pairs, 2, behind, 4)),
            dma((pairs, near, 2)), dma((pairs, near, 2)), dma((n_tp - 1, 2)), dma((n_tp - 1, 2)),
        ],
        compiler_params=pltpu.CompilerParams(
            vmem_limit_bytes=63 * 1024 * 1024, collective_id=0, has_side_effects=True
        ),
        name="layer_core",
    )(hidden, gain, freq, wq, wk, wv, wo, post)


def body(mesh, hidden_in, pre_gain, query_proj, key_proj, value_proj, out_proj, post_gain):
    rows, depth = hidden_in.shape
    width = query_proj.shape[1]
    group = group_of(mesh, width)
    all_rows = rows * group
    behind = -(-(WIDE * SPAN) // all_rows)
    half_dim = HEAD_DIM // 2
    frequency = ROPE_BASE ** (-(jnp.arange(half_dim, dtype=jnp.float32) * 2.0 / HEAD_DIM))
    freq = jnp.concatenate([frequency] * (LANES // half_dim))[None, :]
    return layer(
        mesh, group, behind, hidden_in, pre_gain[None, :], freq,
        query_proj, key_proj, value_proj, out_proj, post_gain[None, :],
    )


def solution(mesh):
    placed = (P("sp", None), P(), P(None, "tp"), P("sp", "tp"), P("sp", "tp"), P("tp", None), P())
    return jax.shard_map(
        functools.partial(body, mesh),
        mesh=mesh,
        in_specs=placed,
        out_specs=(P(("sp", "tp"), None), P("tp", "sp")),
        check_vma=False,
    )
```

time: 136 us -> 112 us (0.82)
  Pallas kernels: 124 us -> 106 us
  matrix products: 6.19 us -> 0 us
  other arithmetic: 3.83 us -> 0.6 us
  local copies, waits for them, and re-layouts: 1.41 us -> 3.68 us
    pallas_call x3 -> x1, Pallas kernels: 124 us -> 106 us  [layer(): pl.pallas_call(functools.partial(layer_kernel, n_sp, n_tp, group, behind)...]
    dot_general x1 -> x0, matrix products: 6.19 us -> none  [body(): jnp.dot(attended, out_proj, preferred_element_type=jnp.float32)]
    unnamed x6 -> x2, local copies, waits for them, and re-layouts: 0.01 us -> 3.68 us
    reduce_sum x1 -> x0, other arithmetic: 1.74 us -> none  [body(): scale = lax.rsqrt(jnp.mean(summed * summed, axis=-1, keepdims=True) + EPS)]
    convert_element_type x1 -> x0, other arithmetic: 1.48 us -> none  [body(): layer_out = (summed * scale * post_gain).astype(jnp.bfloat16)]
    reshape x1 -> x0, local copies, waits for them, and re-layouts: 1.4 us -> none  [body(): return (layer_out, log_weight.reshape(width // HEAD_DIM, rows))]
where the time goes in v2:
time: 112 us; the launch traced here: 111 us
  Pallas kernels  106 us (95%)
  local copies, waits for them, and re-layouts  3.68 us (3%)
    pallas_call x1, Pallas kernels, layer(): pl.pallas_call(functools.partial(layer_kernel, n_sp, n_tp, group, behind)...  106 us
    unnamed x2, local copies, waits for them, and re-layouts  3.68 us

profile of v2, /device:TPU:9, one launch (start us, length us, event | category | flops | bytes accessed | tf_op | source)
XLA Modules:
  0.0 111.4 jit_solution(14420055626280654089)
XLA Ops:
  0.6 0.6 maximum_bitcast_fusion.freq_ref
  1.2 106.5 %layer_core.1 = (bf16[256,2048]{1,0:T(8,128)(2,1)}, f32[16,512]{1,0:T(8,128)}) custom-call(bf16[512,2048]{1,0:T(8,128)(2,1)} %hid_ref.1, f32[1,2048]{1,0:T(1,128)} %bitcast.4, f32[1,128]{1,0:T(1,128)} %maximum_bitcast_fusion.freq_ref, bf16[2048,1024]{1,0:T(8,128)(2,1)} %wq_ref.1, bf16[128,1024]{1,0:T(8,128)(2,1)} %wk_ref.1, bf16[128,1024]{1,0:T(8,128)(2,1)} %wv_ref.1, ...), custom_call_target="tpu_custom_call" | custom-call | tf_op jit(solution)/shard_map/layer_core/pallas_call | solution.py:621
  107.7 2.3 %copy.11 = bf16[256,2048]{1,0:T(8,128)(2,1)} copy(bf16[256,2048]{1,0:T(8,128)(2,1)} %get-tuple-element.4) | data formatting | bytes 2097152
  110.0 1.4 %copy.12 = f32[16,512]{1,0:T(8,128)} copy(f32[16,512]{1,0:T(8,128)} %get-tuple-element.5) | data formatting | bytes 65536
  (1 shorter events, 0.0 us)

commit v3 on v2

--- a/solution.py
+++ b/solution.py
@@ -224,7 +224,12 @@
         return 4 * (a % 32 + 32 - b % 64) + a // 32 - b // 64, b % 64 - 32
 
     put_bias(b1, plain, g * all_rows)
-    put_bias(b16, plain, g * steps)
+    a16 = lax.broadcasted_iota(jnp.int32, (few, few + SPAN), 0)
+    k16 = lax.broadcasted_iota(jnp.int32, (few, few + SPAN), 1)
+    for i in range(group):
+        band = (a16 + SPAN >= k16) & (a16 <= k16)
+        seen = g * steps + i * few + k16 >= SPAN
+        b16[i] = jnp.where(band & seen, 0.0, NEG).astype(f32)
     put_bias(b4, woven, g * steps)
 
     for k, q in firsts + seconds:
@@ -299,13 +304,13 @@
             early_s.at[pair, j], early_r.at[pair, j], (after[0], t),
         )
 
-    def late(pair, j, k, b):
+    def late(pair, j, block, b):
         ref = (kx_all, vx_all)[j]
-        at = pl.multiple_of(flip(c, k) * few, few)
+        at = pl.multiple_of(block * few, few)
         return remote(
             ref.at[pair, :, pl.ds(behind * steps + at, few)],
             ref.at[pair, :, pl.ds((behind - b) * steps + at, few)],
-            late_s.at[pair, j, b - 1, k], late_r.at[pair, j, b - 1, k], (after[b - 1], t),
+            late_s.at[pair, j, b - 1, block], late_r.at[pair, j, b - 1, block], (after[b - 1], t),
         )
 
     everything = [0] + masks
@@ -314,7 +319,7 @@
         for b in range(1, behind + 1):
             @pl.when(g + b < count)
             def _(b=b):
-                late(pair, j, k, b).start()
+                late(pair, j, flip(c, k), b).start()
 
     def send_early(pair, j):
         @pl.when(g + 1 < count)
@@ -346,25 +351,16 @@
     for j in range(2):
         send_early(0, j)
 
-    def part_of(pair, j, u, b):
-        ref = (kx_all, vx_all)[j]
-        return remote(
-            ref.at[pair, pl.ds(4 * u, 4), pl.ds(behind * steps, steps)],
-            ref.at[pair, pl.ds(4 * u, 4), pl.ds((behind - b) * steps, steps)],
-            late_s.at[pair, j, b - 1, u], late_r.at[pair, j, b - 1, u], (after[b - 1], t),
-        )
-
     for pair in range(1, pairs):
         for j in range(2):
             send_early(pair, j)
-        for u in range(4):
-            for j in range(2):
-                for b in range(1, behind + 1):
-                    @pl.when(g + b < count)
-                    def _(pair=pair, j=j, u=u, b=b):
-                        part_of(pair, j, u, b).start()
-
-    block = min(SPAN, steps)
+        for block in range(group)[::-1]:
+            for b in range(1, behind + 1):
+                @pl.when(g + b < count)
+                def _(pair=pair, block=block, b=b):
+                    for j in range(2):
+                        late(pair, j, block, b).start()
+
     skip16 = behind * steps - SPAN
 
     def tile(q, k, v, bias):
@@ -384,23 +380,32 @@
             jnp.where(low, o[:n, LANES:], o[n:, LANES:]),
         )
 
-    blocks16 = steps // block
     blocks4 = steps // 32
 
-    def back(p, k):
-        to = (peer[k], t)
-        span = pl.ds(pl.multiple_of(flip(c, k) * rows, rows), rows)
+    def back(p, block):
+        to = (base + block, t)
+        span = pl.ds(block * rows, rows)
         mine = pl.ds(pl.multiple_of(c * LANES, LANES), LANES)
         return (
-            remote(att.at[p, span], att_in.at[p, :, mine], back_s.at[p, k - 1, 0], back_r.at[p, k - 1, 0], to),
-            remote(lw.at[p, :, span], lw_in.at[c, p], back_s.at[p, k - 1, 1], back_r.at[p, k - 1, 1], to),
+            remote(att.at[p, span], att_in.at[p, :, mine], back_s.at[p, block, 0], back_r.at[p, c, 0], to),
+            remote(lw.at[p, :, span], lw_in.at[c, p], back_s.at[p, block, 1], back_r.at[p, c, 1], to),
+        )
+
+    def back_in(p, k):
+        of = flip(c, k)
+        theirs = pl.ds(pl.multiple_of(of * LANES, LANES), LANES)
+        return (
+            remote(
+                att_in.at[p, :, theirs], att_in.at[p, :, theirs], back_s.at[p, 0, 0], back_r.at[p, of, 0], (peer[k], t)
+            ),
+            remote(lw_in.at[of, p], lw_in.at[of, p], back_s.at[p, 0, 1], back_r.at[p, of, 1], (peer[k], t)),
         )
 
     def mix_out(p):
         for copy in kept[4 + p * group:4 + (p + 1) * group]:
             copy.wait()
         for k in masks:
-            for copy in back(p, k):
+            for copy in back_in(p, k):
                 copy.wait_recv()
         value = jnp.dot(att_in[p], wo[p], preferred_element_type=f32)
         total[...] = value if p == 0 else total[...] + value
@@ -408,17 +413,13 @@
     for p in range(pairs):
         qn, kw, vw, qr, kx, vx = (ref.at[p] for ref in (qn_all, kw_all, vw_all, qr_all, kx_all, vx_all))
 
-        def step16(idx, _):
-            slot = idx // blocks16
-            i = idx % blocks16
+        def step16(block, slot):
             r = 4 * (slot % 4) + slot // 4
-            at = pl.multiple_of(i * block, block)
-            keys = pl.ds(at + skip16, block + SPAN)
-            got = tile(
-                qr[slot, pl.ds(at, block), :], kx[slot, keys, :], vx[slot, keys, :], b16[jnp.minimum(i, 1)]
-            )
+            at = block * few
+            keys = pl.ds(at + skip16, few + SPAN)
+            got = tile(qr[slot, pl.ds(at, few), :], kx[slot, keys, :], vx[slot, keys, :], b16[block])
             for ref, value in zip((acc16, m16, l16), got):
-                ref[pl.ds(r + WIDE * at, block, stride=WIDE), :] = value
+                ref[pl.ds(r + WIDE * at, few, stride=WIDE), :] = value
             return 0
 
         def step4(r, i):
@@ -464,45 +465,37 @@
         if blocks4 > 1:
             lax.fori_loop(
                 0, 4 * (blocks4 - 1),
-                lambda idx, _: step4(idx // (blocks4 - 1), idx % (blocks4 - 1) + 1), 0, unroll=2,
+                lambda idx, _: step4(idx // (blocks4 - 1), idx % (blocks4 - 1) + 1), 0, unroll=4,
             )
-        lax.fori_loop(1, all_rows // SPAN, step1, 0, unroll=2)
-        for j in range(2):
-            @pl.when(g >= 1)
-            def _(j=j):
-                early(p, j).wait_recv()
-        step1(0, 0)
+        plains = all_rows // SPAN - 1
+        lax.fori_loop(1, plains + 1, step1, 0, unroll=max(x for x in range(1, 6) if plains % x == 0))
         if p > 0:
             mix_out(p - 1)
-        if p == 0:
-            for j in range(2):
-                for b in range(1, behind + 1):
-                    @pl.when(g >= b)
-                    def _(j=j, b=b):
-                        for k in everything:
-                            late(0, j, k, b).wait_recv()
-            lax.fori_loop(0, 4, lambda r, _: step4(r, 0), 0, unroll=2)
-            lax.fori_loop(0, WIDE * blocks16, step16, 0, unroll=2)
-        else:
-            def chunk(u, _):
+        tiles = rows // SPAN
+        for block in range(group)[::-1]:
+            for b in range(1, behind + 1):
+                for h in range(group):
+                    age = (behind - b) * group + h
+                    if age == block or (block == group - 1 and age > block):
+                        @pl.when(g >= b)
+                        def _(b=b, h=h):
+                            for j in range(2):
+                                late(p, j, h, b).wait_recv()
+            if block == group - 1:
+                lax.fori_loop(0, 4, lambda r, _: step4(r, 0), 0, unroll=4)
                 for j in range(2):
-                    for b in range(1, behind + 1):
-                        @pl.when(g >= b)
-                        def _(j=j, b=b):
-                            part_of(p, j, u, b).wait_recv()
-                step4(u, 0)
-                lax.fori_loop(0, 4 * blocks16, lambda n, _: step16(4 * blocks16 * u + n, 0), 0, unroll=2)
-                return 0
-
-            lax.fori_loop(0, 4, chunk, 0)
-        order = masks[::-1] + [0]
-        tiles = rows // SPAN
-        for i, k in enumerate(order):
-            first = flip(c, k) * tiles
-            lax.fori_loop(0, tiles, lambda n, _: merge(first + n, 0), 0, unroll=2)
-            if i > 0:
-                for copy in back(p, order[i - 1]):
+                    @pl.when(g >= 1)
+                    def _(j=j):
+                        early(p, j).wait_recv()
+                step1(0, 0)
+            lax.fori_loop(0, WIDE, lambda n, _, block=block: step16(block, n), 0, unroll=4)
+            lax.fori_loop(0, tiles, lambda n, _, block=block: merge(block * tiles + n, 0), 0, unroll=4)
+
+            @pl.when(c != block)
+            def _(block=block):
+                for copy in back(p, block):
                     copy.start()
+
         here = pl.ds(start_row, rows)
         mine = pl.ds(pl.multiple_of(c * LANES, LANES), LANES)
         att_in[p, :, mine] = att[p, here, :]
@@ -512,7 +505,7 @@
     for copy in kept[4 + last * group:]:
         copy.wait()
     for k in masks:
-        for copy in back(last, k):
+        for copy in back_in(last, k):
             copy.wait_recv()
     share = rows // n_tp
     sub = share // 2
@@ -562,9 +555,11 @@
         for i in range(2):
             swap(k, i).wait_send()
     for p in range(pairs):
-        for k in masks:
-            for copy in back(p, k):
-                copy.wait_send()
+        for block in range(group):
+            @pl.when(c != block)
+            def _(p=p, block=block):
+                for copy in back(p, block):
+                    copy.wait_send()
     for j in range(2):
         for k in masks:
             near(k, j).wait_send()
@@ -588,12 +583,8 @@
             for b in range(1, behind + 1):
                 @pl.when(g + b < count)
                 def _(pair=pair, j=j, b=b):
-                    if pair == 0:
-                        for k in everything:
-                            late(pair, j, k, b).wait_send()
-                    else:
-                        for u in range(4):
-                            part_of(pair, j, u, b).wait_send()
+                    for block in range(group):
+                        late(pair, j, block, b).wait_send()
 
 
 def layer(mesh, group, behind, hidden, gain, freq, wq, wk, wv, wo, post):
@@ -605,7 +596,7 @@
     pairs = part // LANES
     all_rows = rows * group
     steps = all_rows // WIDE
-    block = min(SPAN, steps)
+    few = rows // WIDE
     count = n_sp // group
     share = rows // n_tp
     f32, bf16 = jnp.float32, jnp.bfloat16
@@ -635,7 +626,7 @@
             state, state, state, state, state, state, state, state, state,
             pltpu.VMEM((2, SPAN, 2 * SPAN), f32),
             pltpu.VMEM((2, SPAN, 2 * SPAN), f32),
-            pltpu.VMEM((2, block, block + SPAN), f32),
+            pltpu.VMEM((group, few, few + SPAN), f32),
             pltpu.VMEM((pairs, all_rows, LANES), bf16), pltpu.VMEM((pairs, rows, group * LANES), bf16),
             pltpu.VMEM((pairs, 2, all_rows), f32), pltpu.VMEM((group, pairs, 2, rows), f32),
             pltpu.VMEM((rows, depth), f32), pieces, pieces,
@@ -643,8 +634,8 @@
             dma((2, near)), dma((2, near)), dma((2, 2, count)), dma((2, 2, count)),
             dma((2, 2)), dma((2, 2)), dma((2,)), dma((2,)), dma((3, 2)), dma((3, 2)),
             dma((pairs, 2)), dma((pairs, 2)),
-            dma((pairs, 2, behind, 4)), dma((pairs, 2, behind, 4)),
-            dma((pairs, near, 2)), dma((pairs, near, 2)), dma((n_tp - 1, 2)), dma((n_tp - 1, 2)),
+            dma((pairs, 2, behind, group)), dma((pairs, 2, behind, group)),
+            dma((pairs, group, 2)), dma((pairs, group, 2)), dma((n_tp - 1, 2)), dma((n_tp - 1, 2)),
         ],
         compiler_params=pltpu.CompilerParams(
             vmem_limit_bytes=63 * 1024 * 1024, collective_id=0, has_side_effects=True

time: 112 us -> 133 us (1.19)
  Pallas kernels: 106 us -> 128 us
    pallas_call x1, Pallas kernels: 106 us -> 128 us  [layer(): pl.pallas_call(functools.partial(layer_kernel, n_sp, n_tp, group, behind)...]
where the time goes in v3:
time: 133 us
  Pallas kernels  128 us (96%)
  local copies, waits for them, and re-layouts  3.68 us (3%)
    pallas_call x1, Pallas kernels, layer(): pl.pallas_call(functools.partial(layer_kernel, n_sp, n_tp, group, behind)...  128 us
    unnamed x2, local copies, waits for them, and re-layouts  3.68 us

profile of v3, /device:TPU:9, one launch (start us, length us, event | category | flops | bytes accessed | tf_op | source)
XLA Modules:
  0.0 133.1 jit_solution(14146970684835135174)
XLA Ops:
  0.6 0.6 maximum_bitcast_fusion.freq_ref
  1.2 128.2 %layer_core.1 = (bf16[256,2048]{1,0:T(8,128)(2,1)}, f32[16,512]{1,0:T(8,128)}) custom-call(bf16[512,2048]{1,0:T(8,128)(2,1)} %hid_ref.1, f32[1,2048]{1,0:T(1,128)} %bitcast.4, f32[1,128]{1,0:T(1,128)} %maximum_bitcast_fusion.freq_ref, bf16[2048,1024]{1,0:T(8,128)(2,1)} %wq_ref.1, bf16[128,1024]{1,0:T(8,128)(2,1)} %wk_ref.1, bf16[128,1024]{1,0:T(8,128)(2,1)} %wv_ref.1, ...), custom_call_target="tpu_custom_call" | custom-call | tf_op jit(solution)/shard_map/layer_core/pallas_call | solution.py:612
  129.4 2.3 %copy.11 = bf16[256,2048]{1,0:T(8,128)(2,1)} copy(bf16[256,2048]{1,0:T(8,128)(2,1)} %get-tuple-element.4) | data formatting | bytes 2097152
  131.7 1.4 %copy.12 = f32[16,512]{1,0:T(8,128)} copy(f32[16,512]{1,0:T(8,128)} %get-tuple-element.5) | data formatting | bytes 65536
  (1 shorter events, 0.0 us)

commit v4 on v2

--- a/solution.py
+++ b/solution.py
@@ -46,10 +46,10 @@
     out_ref, lw_ref,
     raw, nrm, wq, wk, wv, wo, cos_t, sin_t, scr,
     qn_all, kw_all, vw_all, qr_all, kx_all, vx_all,
-    acc1, m1, l1, acc4, m4, l4, acc16, m16, l16, b1, b4, b16,
-    att, att_in, lw, lw_in, total, snd, rcv,
+    acc1, m1, l1, acc4, m4, l4, wide, b1, b4, b16,
+    att, att_in, lw, lw_in, total, mix, keep, snd, rcv, final,
     local, near_s, near_r, line_s, line_r, dir_s, dir_r, across_s, across_r, twin_s, twin_r,
-    early_s, early_r, late_s, late_r, back_s, back_r, swap_s, swap_r,
+    early_s, early_r, late_s, late_r, back_s, back_r, level_s, level_r, swap_s, swap_r,
 ):
     f32, bf16 = jnp.float32, jnp.bfloat16
     s = lax.axis_index("sp")
@@ -224,7 +224,10 @@
         return 4 * (a % 32 + 32 - b % 64) + a // 32 - b // 64, b % 64 - 32
 
     put_bias(b1, plain, g * all_rows)
-    put_bias(b16, plain, g * steps)
+    a16 = lax.broadcasted_iota(jnp.int32, b16.shape, 0)
+    k16 = lax.broadcasted_iota(jnp.int32, b16.shape, 1)
+    seen = (a16 + SPAN >= k16) & (a16 <= k16) & (g * steps + k16 >= SPAN)
+    b16[...] = jnp.where(seen, 0.0, NEG).astype(f32)
     put_bias(b4, woven, g * steps)
 
     for k, q in firsts + seconds:
@@ -364,7 +367,6 @@
                     def _(pair=pair, j=j, u=u, b=b):
                         part_of(pair, j, u, b).start()
 
-    block = min(SPAN, steps)
     skip16 = behind * steps - SPAN
 
     def tile(q, k, v, bias):
@@ -384,41 +386,116 @@
             jnp.where(low, o[:n, LANES:], o[n:, LANES:]),
         )
 
-    blocks16 = steps // block
     blocks4 = steps // 32
 
-    def back(p, k):
-        to = (peer[k], t)
+    mine = pl.ds(pl.multiple_of(c * LANES, LANES), LANES)
+    own_steps = pl.ds(pl.multiple_of(c * few, few), few)
+
+    def back(p, k, u):
+        slots = pl.ds(4 * u, 4)
+        span = pl.ds(pl.multiple_of(flip(c, k) * few, few), few)
+        return remote(
+            att.at[p, slots, span], att_in.at[p, slots, :, mine],
+            back_s.at[p, k - 1, u], back_r.at[p, k - 1, u], (peer[k], t),
+        )
+
+    def level(p, k):
         span = pl.ds(pl.multiple_of(flip(c, k) * rows, rows), rows)
-        mine = pl.ds(pl.multiple_of(c * LANES, LANES), LANES)
-        return (
-            remote(att.at[p, span], att_in.at[p, :, mine], back_s.at[p, k - 1, 0], back_r.at[p, k - 1, 0], to),
-            remote(lw.at[p, :, span], lw_in.at[c, p], back_s.at[p, k - 1, 1], back_r.at[p, k - 1, 1], to),
-        )
-
-    def mix_out(p):
+        return remote(lw.at[p, :, span], lw_in.at[c, p], level_s.at[p, k - 1], level_r.at[p, k - 1], (peer[k], t))
+
+    def send_back(p, u):
+        for k in masks[::-1]:
+            back(p, k, u).start()
+        slots = pl.ds(4 * u, 4)
+        att_in[p, slots, :, mine] = att[p, slots, own_steps, :]
+
+    def levels(p):
+        def turn(i, _):
+            here = pl.ds(pl.multiple_of(i * SPAN, SPAN), SPAN)
+            turned = jnp.transpose(wide[here, :])
+            lw[p, 0:1, here] = turned[0:1]
+            lw[p, 1:2, here] = turned[HEAD_DIM:HEAD_DIM + 1]
+            return 0
+
+        lax.fori_loop(0, all_rows // SPAN, turn, 0, unroll=4)
+
+    def send_levels(p):
+        for k in masks:
+            level(p, k).start()
+        lw_in[c, p] = lw[p, :, pl.ds(start_row, rows)]
+
+    def fetched(p):
         for copy in kept[4 + p * group:4 + (p + 1) * group]:
             copy.wait()
+
+    def mix_out(p):
+        fetched(p)
         for k in masks:
-            for copy in back(p, k):
-                copy.wait_recv()
-        value = jnp.dot(att_in[p], wo[p], preferred_element_type=f32)
-        total[...] = value if p == 0 else total[...] + value
+            for u in range(4):
+                back(p, k, u).wait_recv()
+        for u in range(4):
+            rows_in = att_in[p, pl.ds(4 * u, 4)].reshape(4 * few, group * LANES)
+            value = jnp.dot(rows_in, wo[p], preferred_element_type=f32)
+            total[u] = value if p == 0 else total[u] + value
+
+    last = pairs - 1
+    thin = few // n_tp
+
+    def swap(k, u):
+        return remote(
+            snd.at[k - 1, u], rcv.at[k - 1, u], swap_s.at[k - 1, u], swap_r.at[k - 1, u],
+            (s, lax.rem(t + k, n_tp)),
+        )
+
+    def share_of(owner):
+        if thin % 8 == 0:
+            return mix[:, pl.ds(pl.multiple_of(owner * thin, thin), thin), :].astype(bf16)
+        value = mix[:, 0:thin, :]
+        for o in range(1, n_tp):
+            value = jnp.where(owner == o, mix[:, o * thin:(o + 1) * thin, :], value)
+        return value.astype(bf16)
+
+    def close(u):
+        for k in masks:
+            back(last, k, u).wait_recv()
+        rows_in = att_in[last, pl.ds(4 * u, 4)].reshape(4 * few, group * LANES)
+        value = jnp.dot(rows_in, wo[last], preferred_element_type=f32)
+        if last > 0:
+            value = value + total[u]
+        mix[...] = value.reshape(4, few, value.shape[1])
+        for k in range(1, n_tp):
+            snd[k - 1, u] = share_of(lax.rem(t + k, n_tp))
+        keep[u] = share_of(t)
+        for k in range(1, n_tp):
+            swap(k, u).start()
+
+    def settle(u):
+        value = keep[u].astype(f32)
+        for k in range(1, n_tp):
+            swap(k, u).wait_recv()
+            value = value + rcv[k - 1, u].astype(f32)
+        scale = lax.rsqrt(jnp.mean(value * value, axis=-1, keepdims=True) + EPS)
+        value = value * scale * post_ref[...]
+        for j in range(4):
+            for i in range(depth // LANES):
+                final[i, pl.ds(u + 4 * j, thin, stride=WIDE), :] = value[j, :, i * LANES:(i + 1) * LANES]
 
     for p in range(pairs):
         qn, kw, vw, qr, kx, vx = (ref.at[p] for ref in (qn_all, kw_all, vw_all, qr_all, kx_all, vx_all))
 
-        def step16(idx, _):
-            slot = idx // blocks16
-            i = idx % blocks16
+        def step16(slot, _):
             r = 4 * (slot % 4) + slot // 4
-            at = pl.multiple_of(i * block, block)
-            keys = pl.ds(at + skip16, block + SPAN)
-            got = tile(
-                qr[slot, pl.ds(at, block), :], kx[slot, keys, :], vx[slot, keys, :], b16[jnp.minimum(i, 1)]
-            )
-            for ref, value in zip((acc16, m16, l16), got):
-                ref[pl.ds(r + WIDE * at, block, stride=WIDE), :] = value
+            keys = pl.ds(skip16, steps + SPAN)
+            o16, m16, l16 = tile(qr[slot], kx[slot, keys, :], vx[slot, keys, :], b16[...])
+            apart = pl.ds(r, steps, stride=WIDE)
+            here = pl.ds(pl.multiple_of(slot * steps, steps), steps)
+            m_1, m_4 = m1[apart, :], m4[here, :]
+            top = jnp.maximum(m16, jnp.maximum(m_1, m_4))
+            e1, e4, e16 = jnp.exp(m_1 - top), jnp.exp(m_4 - top), jnp.exp(m16 - top)
+            whole = l1[apart, :] * e1 + l4[here, :] * e4 + l16 * e16
+            mixed = acc1[apart, :] * e1 + acc4[here, :] * e4 + o16 * e16
+            att[p, slot] = (mixed / whole).astype(bf16)
+            wide[apart, :] = top + jnp.log(whole)
             return 0
 
         def step4(r, i):
@@ -436,7 +513,7 @@
             )
             for ref, value in zip((acc4, m4, l4), got):
                 for j in range(4):
-                    ref[pl.ds(r + 4 * j + WIDE * at, 32, stride=WIDE), :] = value[j * 32:(j + 1) * 32]
+                    ref[pl.ds(pl.multiple_of((4 * r + j) * steps + at, 32), 32), :] = value[j * 32:(j + 1) * 32]
             return 0
 
         def step1(i, _):
@@ -448,25 +525,13 @@
                 ref[here, :] = value
             return 0
 
-        def merge(i, _):
-            here = pl.ds(pl.multiple_of(i * SPAN, SPAN), SPAN)
-            tops = (m1[here, :], m4[here, :], m16[here, :])
-            top = jnp.maximum(tops[0], jnp.maximum(tops[1], tops[2]))
-            e1, e4, e16 = (jnp.exp(x - top) for x in tops)
-            whole = l1[here, :] * e1 + l4[here, :] * e4 + l16[here, :] * e16
-            mixed = acc1[here, :] * e1 + acc4[here, :] * e4 + acc16[here, :] * e16
-            att[p, here, :] = (mixed / whole).astype(bf16)
-            turned = jnp.transpose(top + jnp.log(whole))
-            lw[p, 0:1, here] = turned[0:1]
-            lw[p, 1:2, here] = turned[HEAD_DIM:HEAD_DIM + 1]
-            return 0
-
         if blocks4 > 1:
             lax.fori_loop(
                 0, 4 * (blocks4 - 1),
-                lambda idx, _: step4(idx // (blocks4 - 1), idx % (blocks4 - 1) + 1), 0, unroll=2,
+                lambda idx, _: step4(idx // (blocks4 - 1), idx % (blocks4 - 1) + 1), 0, unroll=4,
             )
-        lax.fori_loop(1, all_rows // SPAN, step1, 0, unroll=2)
+        plains = all_rows // SPAN - 1
+        lax.fori_loop(1, plains + 1, step1, 0, unroll=max(x for x in range(1, 6) if plains % x == 0))
         for j in range(2):
             @pl.when(g >= 1)
             def _(j=j):
@@ -474,6 +539,8 @@
         step1(0, 0)
         if p > 0:
             mix_out(p - 1)
+        if p == last:
+            fetched(last)
         if p == 0:
             for j in range(2):
                 for b in range(1, behind + 1):
@@ -481,90 +548,46 @@
                     def _(j=j, b=b):
                         for k in everything:
                             late(0, j, k, b).wait_recv()
-            lax.fori_loop(0, 4, lambda r, _: step4(r, 0), 0, unroll=2)
-            lax.fori_loop(0, WIDE * blocks16, step16, 0, unroll=2)
-        else:
-            def chunk(u, _):
+        for u in range(4):
+            if p > 0:
                 for j in range(2):
                     for b in range(1, behind + 1):
                         @pl.when(g >= b)
-                        def _(j=j, b=b):
+                        def _(j=j, b=b, u=u):
                             part_of(p, j, u, b).wait_recv()
-                step4(u, 0)
-                lax.fori_loop(0, 4 * blocks16, lambda n, _: step16(4 * blocks16 * u + n, 0), 0, unroll=2)
-                return 0
-
-            lax.fori_loop(0, 4, chunk, 0)
-        order = masks[::-1] + [0]
-        tiles = rows // SPAN
-        for i, k in enumerate(order):
-            first = flip(c, k) * tiles
-            lax.fori_loop(0, tiles, lambda n, _: merge(first + n, 0), 0, unroll=2)
-            if i > 0:
-                for copy in back(p, order[i - 1]):
-                    copy.start()
-        here = pl.ds(start_row, rows)
-        mine = pl.ds(pl.multiple_of(c * LANES, LANES), LANES)
-        att_in[p, :, mine] = att[p, here, :]
-        lw_in[c, p] = lw[p, :, here]
-
-    last = pairs - 1
-    for copy in kept[4 + last * group:]:
-        copy.wait()
-    for k in masks:
-        for copy in back(last, k):
-            copy.wait_recv()
-    share = rows // n_tp
-    sub = share // 2
-
-    def finish(owner, i):
-        here = pl.ds(pl.multiple_of(owner * share + i * sub, sub), sub)
-        value = jnp.dot(att_in[last, here, :], wo[last], preferred_element_type=f32)
-        if last > 0:
-            value = value + total[here, :]
-        return value.astype(bf16)
-
-    def swap(k, i):
-        at = pl.ds(i * sub, sub)
-        return remote(
-            snd.at[k - 1, at], rcv.at[k - 1, at], swap_s.at[k - 1, i], swap_r.at[k - 1, i],
-            (s, lax.rem(t + k, n_tp)),
-        )
-
-    waiting = []
-    for k in range(1, n_tp):
-        for i in range(2):
-            snd[k - 1, pl.ds(i * sub, sub), :] = finish(lax.rem(t + k, n_tp), i)
-            if waiting:
-                waiting.pop().start()
-            waiting.append(swap(k, i))
-    for i in range(2):
-        at = pl.ds(i * sub, sub)
-        total[at, :] = finish(t, i).astype(f32)
-        if waiting:
-            waiting.pop().start()
+            step4(u, 0)
+            lax.fori_loop(0, 4, lambda n, _, u=u: step16(4 * u + n, 0), 0, unroll=4)
+            send_back(p, u)
+            if p == last and u >= 1:
+                close(u - 1)
+            if p == last and u >= 2:
+                settle(u - 2)
+        levels(p)
+        send_levels(p)
+
+    close(3)
+    settle(2)
     heads = 2 * pairs
+    for p in range(pairs):
+        for k in masks:
+            level(p, k).wait_recv()
     for i in range(group):
         for p in range(pairs):
             for h in range(2):
                 row = i * heads + p * 2 + h
                 lw_ref[row:row + 1, :] = lw_in[i, p, h:h + 1, :]
-    for i in range(2):
-        at = pl.ds(i * sub, sub)
-        value = total[at, :]
-        for k in range(1, n_tp):
-            swap(k, i).wait_recv()
-            value = value + rcv[k - 1, at, :].astype(f32)
-        scale = lax.rsqrt(jnp.mean(value * value, axis=-1, keepdims=True) + EPS)
-        out_ref[at, :] = (value * scale * post_ref[...]).astype(bf16)
+    settle(3)
+    for i in range(depth // LANES):
+        out_ref[:, i * LANES:(i + 1) * LANES] = final[i].astype(bf16)
 
     for k in range(1, n_tp):
-        for i in range(2):
-            swap(k, i).wait_send()
+        for u in range(4):
+            swap(k, u).wait_send()
     for p in range(pairs):
         for k in masks:
-            for copy in back(p, k):
-                copy.wait_send()
+            level(p, k).wait_send()
+            for u in range(4):
+                back(p, k, u).wait_send()
     for j in range(2):
         for k in masks:
             near(k, j).wait_send()
@@ -605,7 +628,8 @@
     pairs = part // LANES
     all_rows = rows * group
     steps = all_rows // WIDE
-    block = min(SPAN, steps)
+    few = rows // WIDE
+    thin = few // n_tp
     count = n_sp // group
     share = rows // n_tp
     f32, bf16 = jnp.float32, jnp.bfloat16
@@ -615,7 +639,7 @@
     table = pltpu.VMEM((all_rows, LANES), f32)
     ring = pltpu.VMEM((pairs, SPAN + all_rows, LANES), bf16)
     woven = pltpu.VMEM((pairs, WIDE, (behind + 1) * steps, LANES), bf16)
-    pieces = pltpu.VMEM((n_tp - 1, share, depth), bf16)
+    pieces = pltpu.VMEM((n_tp - 1, 4, 4, thin, depth), bf16)
     vmem = pl.BlockSpec(memory_space=pltpu.VMEM)
     near = max(group - 1, 1)
     return pl.pallas_call(
@@ -632,19 +656,22 @@
             pltpu.VMEM((pairs, rows, LANES), f32),
             pltpu.VMEM((pairs, all_rows, LANES), bf16), ring, ring,
             pltpu.VMEM((pairs, WIDE, steps, LANES), bf16), woven, woven,
-            state, state, state, state, state, state, state, state, state,
+            state, state, state, state, state, state, state,
             pltpu.VMEM((2, SPAN, 2 * SPAN), f32),
             pltpu.VMEM((2, SPAN, 2 * SPAN), f32),
-            pltpu.VMEM((2, block, block + SPAN), f32),
-            pltpu.VMEM((pairs, all_rows, LANES), bf16), pltpu.VMEM((pairs, rows, group * LANES), bf16),
+            pltpu.VMEM((steps, steps + SPAN), f32),
+            pltpu.VMEM((pairs, WIDE, steps, LANES), bf16), pltpu.VMEM((pairs, WIDE, few, group * LANES), bf16),
             pltpu.VMEM((pairs, 2, all_rows), f32), pltpu.VMEM((group, pairs, 2, rows), f32),
-            pltpu.VMEM((rows, depth), f32), pieces, pieces,
+            pltpu.VMEM((4, 4 * few, depth), f32), pltpu.VMEM((4, few, depth), f32),
+            pltpu.VMEM((4, 4, thin, depth), bf16), pieces, pieces,
+            pltpu.VMEM((depth // LANES, share, LANES), f32),
             dma((4 + pairs * group,)),
             dma((2, near)), dma((2, near)), dma((2, 2, count)), dma((2, 2, count)),
             dma((2, 2)), dma((2, 2)), dma((2,)), dma((2,)), dma((3, 2)), dma((3, 2)),
             dma((pairs, 2)), dma((pairs, 2)),
             dma((pairs, 2, behind, 4)), dma((pairs, 2, behind, 4)),
-            dma((pairs, near, 2)), dma((pairs, near, 2)), dma((n_tp - 1, 2)), dma((n_tp - 1, 2)),
+            dma((pairs, near, 4)), dma((pairs, near, 4)), dma((pairs, near)), dma((pairs, near)),
+            dma((n_tp - 1, 4)), dma((n_tp - 1, 4)),
         ],
         compiler_params=pltpu.CompilerParams(
             vmem_limit_bytes=63 * 1024 * 1024, collective_id=0, has_side_effects=True

time: 112 us -> 108 us (0.964)
  Pallas kernels: 106 us -> 102 us
    pallas_call x1, Pallas kernels: 106 us -> 102 us  [layer(): pl.pallas_call(functools.partial(layer_kernel, n_sp, n_tp, group, behind)...]
where the time goes in v4:
time: 108 us; the launch traced here: 107 us
  Pallas kernels  102 us (94%)
  local copies, waits for them, and re-layouts  3.68 us (3%)
    pallas_call x1, Pallas kernels, layer(): pl.pallas_call(functools.partial(layer_kernel, n_sp, n_tp, group, behind)...  102 us
    unnamed x2, local copies, waits for them, and re-layouts  3.68 us

profile of v4, /device:TPU:9, one launch (start us, length us, event | category | flops | bytes accessed | tf_op | source)
XLA Modules:
  0.0 107.2 jit_solution(14761904058851925846)
XLA Ops:
  0.6 0.6 maximum_bitcast_fusion.freq_ref
  1.2 102.3 %layer_core.1 = (bf16[256,2048]{1,0:T(8,128)(2,1)}, f32[16,512]{1,0:T(8,128)}) custom-call(bf16[512,2048]{1,0:T(8,128)(2,1)} %hid_ref.1, f32[1,2048]{1,0:T(1,128)} %bitcast.4, f32[1,128]{1,0:T(1,128)} %maximum_bitcast_fusion.freq_ref, bf16[2048,1024]{1,0:T(8,128)(2,1)} %wq_ref.1, bf16[128,1024]{1,0:T(8,128)(2,1)} %wk_ref.1, bf16[128,1024]{1,0:T(8,128)(2,1)} %wv_ref.1, ...), custom_call_target="tpu_custom_call" | custom-call | tf_op jit(solution)/shard_map/layer_core/pallas_call | solution.py:645
  103.5 2.3 %copy.11 = bf16[256,2048]{1,0:T(8,128)(2,1)} copy(bf16[256,2048]{1,0:T(8,128)(2,1)} %get-tuple-element.4) | data formatting | bytes 2097152
  105.8 1.4 %copy.12 = f32[16,512]{1,0:T(8,128)} copy(f32[16,512]{1,0:T(8,128)} %get-tuple-element.5) | data formatting | bytes 65536
  (1 shorter events, 0.0 us)

commit v5 on v4

--- a/solution.py
+++ b/solution.py
@@ -44,11 +44,12 @@
     n_sp, n_tp, group, behind,
     hid_ref, gain_ref, freq_ref, wq_ref, wk_ref, wv_ref, wo_ref, post_ref,
     out_ref, lw_ref,
-    raw, nrm, wq, wk, wv, wo, cos_t, sin_t, scr,
+    raw, nrm, ext, wq, wk, wv, wo, cos_t, sin_t, cos_e, sin_e, scr,
     qn_all, kw_all, vw_all, qr_all, kx_all, vx_all,
-    acc1, m1, l1, acc4, m4, l4, wide, b1, b4, b16,
+    acc1_all, m1_all, l1_all, acc4_all, m4_all, l4_all, wide, b1, b4, b16,
     att, att_in, lw, lw_in, total, mix, keep, snd, rcv, final,
     local, near_s, near_r, line_s, line_r, dir_s, dir_r, across_s, across_r, twin_s, twin_r,
+    rise_s, rise_r, edir_s, edir_r, eacross_s, eacross_r, etwin_s, etwin_r,
     early_s, early_r, late_s, late_r, back_s, back_r, level_s, level_r, swap_s, swap_r,
 ):
     f32, bf16 = jnp.float32, jnp.bfloat16
@@ -75,6 +76,8 @@
     after = [lax.rem(s + b * group, n_sp) for b in range(1, behind + 1)]
     before = [lax.rem(s + n_sp - b * group, n_sp) for b in range(1, behind + 1)]
     start_row = pl.multiple_of(c * rows, rows)
+    mixed = behind == 1 and group == 4
+    end_steps = steps - few if mixed else steps
 
     kept = [pltpu.make_async_copy(hid_ref, raw, local.at[0])]
     own_cols = pl.ds(pl.multiple_of(c * part, LANES), part)
@@ -113,6 +116,17 @@
 
     lax.fori_loop(0, all_rows // LANES, fill, 0)
 
+    def fill_ext(i, _):
+        hi = (base * rows - rows + i * LANES).astype(f32) * freq_ref[...]
+        cos_hi, sin_hi = jnp.cos(hi), jnp.sin(hi)
+        at = pl.ds(pl.multiple_of(i * LANES, LANES), LANES)
+        cos_e[at, :] = cos_lo * cos_hi - sin_lo * sin_hi
+        sin_e[at, :] = (sin_lo * cos_hi + cos_lo * sin_hi) * sign
+        return 0
+
+    if mixed:
+        lax.fori_loop(0, rows // LANES, fill_ext, 0)
+
     @pl.when(g < behind)
     def _():
         for pair in range(pairs):
@@ -188,6 +202,35 @@
         slot = piece(flip(c, k), half, q)
         return remote(slot, slot, twin_s.at[k - 1, q], twin_r.at[k - 1, q], sibling)
 
+    bit = rows // 16
+
+    def rise():
+        at = pl.multiple_of(c * 4 * bit + half * 2 * bit, 2 * bit)
+        src = nrm.at[pl.ds(pl.multiple_of(all_rows - rows + at, 2 * bit), 2 * bit)]
+        return remote(src, ext.at[pl.ds(at, 2 * bit)], rise_s.at[0], rise_r.at[0], (up, t))
+
+    def crumb(block, side, q, n=1):
+        return ext.at[pl.ds(pl.multiple_of(block * 4 * bit + side * 2 * bit + q * bit, bit), n * bit)]
+
+    def ext_direct(k, q):
+        slot = crumb(c, half, q)
+        return remote(slot, slot, edir_s.at[k - 1, q], edir_r.at[k - 1, q], (peer[k], t))
+
+    def ext_across(i):
+        k, other = ((1, 2), (2, 1))[i]
+        slot = crumb(flip(c, k), half, i)
+        return remote(slot, slot, eacross_s.at[i], eacross_r.at[i], (peer[other], t))
+
+    def ext_twin(k, q):
+        slot = crumb(flip(c, k), half, q, 2 if k == 0 else 1)
+        return remote(slot, slot, etwin_s.at[k, q], etwin_r.at[k, q], sibling)
+
+    def share_rise():
+        rise().wait_recv()
+        for k, q in firsts + seconds:
+            ext_direct(k, q).start()
+        ext_twin(0, 0).start()
+
     for j in range(2):
         for k in masks:
             near(k, j).start()
@@ -230,7 +273,7 @@
     b16[...] = jnp.where(seen, 0.0, NEG).astype(f32)
     put_bias(b4, woven, g * steps)
 
-    for k, q in firsts + seconds:
+    for k, q in firsts + seconds[:1]:
         direct(k, q).start()
 
     front = lax.rem(lax.broadcasted_iota(jnp.int32, (rows, LANES), 1), HEAD_DIM) < HEAD_DIM // 2
@@ -261,6 +304,26 @@
             for r in range(WIDE):
                 res[i, 4 * (r % 4) + r // 4, pl.ds(step + skip_res, few), :] = scr[i, pl.ds(r, few, stride=WIDE), :].astype(bf16)
 
+    def project_ext(j):
+        out = jnp.dot(ext[...], (wq, wk, wv)[j][...], preferred_element_type=f32)
+        nat = (qn_all, kw_all, vw_all)[j]
+        res = (qr_all, kx_all, vx_all)[j]
+        for i in range(pairs):
+            u = out[:, i * LANES:(i + 1) * LANES]
+            if j == 1:
+                swapped = jnp.where(
+                    front,
+                    pltpu.roll(u, LANES - HEAD_DIM // 2, 1),
+                    pltpu.roll(u, HEAD_DIM // 2, 1),
+                )
+                u = u * cos_e[...] + swapped * sin_e[...]
+            nat[i, pl.ds(0, SPAN), :] = u[rows - SPAN:].astype(bf16)
+            scr[i] = u
+        for i in range(pairs):
+            for r in range(WIDE):
+                slot = 4 * (r % 4) + r // 4
+                res[i, slot, pl.ds(end_steps, few), :] = scr[i, pl.ds(r, few, stride=WIDE), :].astype(bf16)
+
     for j in range(2):
         for k in masks:
             near(k, j).wait_recv()
@@ -274,20 +337,30 @@
         direct(k, q).wait_recv()
         if group == 4:
             across(k - 1).start()
+            if k == 1:
+                direct(2, 0).start()
         twin(k, q).start()
     if count > 1:
         for j in range(2):
             pass_on(j, 1)
-    for k, q in seconds:
+    for k, q in seconds[:1]:
         direct(k, q).wait_recv()
         twin(k, q).start()
     if count > 2:
         for j in range(2):
             pass_on(j, 2)
-    for k in masks[:2]:
+    for k in masks[:1]:
         for q in range(2):
             twin(k, q).wait_recv()
         project(k, 0)
+    if group == 4:
+        twin(2, 1).wait_recv()
+        if mixed:
+            @pl.when((c != 0) & (g + 1 < count))
+            def _():
+                rise().start()
+        across(0).wait_recv()
+        twin(3, 0).start()
 
     def far(j):
         if count > 3:
@@ -313,9 +386,12 @@
 
     everything = [0] + masks
 
+    def needed(k):
+        return flip(c, k) != group - 1 if mixed else flip(c, k) >= 0
+
     def send_late(pair, j, k):
         for b in range(1, behind + 1):
-            @pl.when(g + b < count)
+            @pl.when((g + b < count) & needed(k))
             def _(b=b):
                 late(pair, j, k, b).start()
 
@@ -326,40 +402,56 @@
 
     for j in range(2):
         far(j)
-        for i, k in enumerate(everything[:3]):
+        if group == 4 and j == 0:
+            twin(3, 0).wait_recv()
+            if mixed:
+                @pl.when((c == 0) & (g + 1 < count))
+                def _():
+                    rise().start()
+        for i, k in enumerate(everything[:2]):
             project(k, 1 + j)
             if i > 0:
                 send_late(0, j, k - 1)
             elif j == 1:
-                send_late(0, 0, everything[:3][-1])
+                send_late(0, 0, everything[:2][-1])
     if group == 4:
-        for k, q in thirds:
-            across(q).wait_recv()
-            twin(k, q).start()
+        direct(2, 0).wait_recv()
+        twin(2, 0).start()
+        across(1).wait_recv()
+        twin(3, 1).start()
+        send_late(0, 1, 1)
+        twin(2, 0).wait_recv()
+        project(2, 1)
+        project(2, 2)
+        if mixed:
+            pl.when(g >= 1)(share_rise)
+        send_late(0, 0, 2)
+        twin(3, 1).wait_recv()
+        project(3, 1)
         send_late(0, 1, 2)
-        for q in range(2):
-            twin(3, q).wait_recv()
-        project(3, 1)
         project(3, 2)
         send_late(0, 0, 3)
+        project(2, 0)
         project(3, 0)
         send_late(0, 1, 3)
     else:
         send_late(0, 1, everything[-1])
-    for j in range(2):
-        send_early(0, j)
+    if not mixed:
+        for j in range(2):
+            send_early(0, j)
 
     def part_of(pair, j, u, b):
         ref = (kx_all, vx_all)[j]
         return remote(
-            ref.at[pair, pl.ds(4 * u, 4), pl.ds(behind * steps, steps)],
-            ref.at[pair, pl.ds(4 * u, 4), pl.ds((behind - b) * steps, steps)],
+            ref.at[pair, pl.ds(4 * u, 4), pl.ds(behind * steps, end_steps)],
+            ref.at[pair, pl.ds(4 * u, 4), pl.ds((behind - b) * steps, end_steps)],
             late_s.at[pair, j, b - 1, u], late_r.at[pair, j, b - 1, u], (after[b - 1], t),
         )
 
     for pair in range(1, pairs):
-        for j in range(2):
-            send_early(pair, j)
+        if not mixed:
+            for j in range(2):
+                send_early(pair, j)
         for u in range(4):
             for j in range(2):
                 for b in range(1, behind + 1):
@@ -480,8 +572,10 @@
             for i in range(depth // LANES):
                 final[i, pl.ds(u + 4 * j, thin, stride=WIDE), :] = value[j, :, i * LANES:(i + 1) * LANES]
 
-    for p in range(pairs):
+    def tiles_of(p):
         qn, kw, vw, qr, kx, vx = (ref.at[p] for ref in (qn_all, kw_all, vw_all, qr_all, kx_all, vx_all))
+        acc1, m1, l1 = (ref.at[p] for ref in (acc1_all, m1_all, l1_all))
+        acc4, m4, l4 = (ref.at[p] for ref in (acc4_all, m4_all, l4_all))
 
         def step16(slot, _):
             r = 4 * (slot % 4) + slot // 4
@@ -525,28 +619,69 @@
                 ref[here, :] = value
             return 0
 
-        if blocks4 > 1:
-            lax.fori_loop(
-                0, 4 * (blocks4 - 1),
-                lambda idx, _: step4(idx // (blocks4 - 1), idx % (blocks4 - 1) + 1), 0, unroll=4,
-            )
-        plains = all_rows // SPAN - 1
-        lax.fori_loop(1, plains + 1, step1, 0, unroll=max(x for x in range(1, 6) if plains % x == 0))
-        for j in range(2):
-            @pl.when(g >= 1)
-            def _(j=j):
-                early(p, j).wait_recv()
+        def rest4():
+            if blocks4 > 1:
+                lax.fori_loop(
+                    0, 4 * (blocks4 - 1),
+                    lambda idx, _: step4(idx // (blocks4 - 1), idx % (blocks4 - 1) + 1), 0, unroll=4,
+                )
+
+        def rest1():
+            plains = all_rows // SPAN - 1
+            lax.fori_loop(1, plains + 1, step1, 0, unroll=max(x for x in range(1, 6) if plains % x == 0))
+
+        return rest4, rest1, step4, step1, step16
+
+    work = [tiles_of(p) for p in range(pairs)]
+
+    def ext_first():
+        for k, q in firsts:
+            ext_direct(k, q).wait_recv()
+            ext_across(k - 1).start()
+            ext_twin(k, q).start()
+
+    def ext_second():
+        for k, q in seconds:
+            ext_direct(k, q).wait_recv()
+            ext_twin(k, q).start()
+
+    def ext_third():
+        for k, q in thirds:
+            ext_across(q).wait_recv()
+            ext_twin(k, q).start()
+        ext_twin(0, 0).wait_recv()
+        for k in masks:
+            for q in range(2):
+                ext_twin(k, q).wait_recv()
+        for j in (1, 2):
+            project_ext(j)
+
+    stages = []
+    if mixed:
+        stages = [ext_first, ext_second, ext_third]
+    for p in range(pairs):
+        for part_work in work[p][:2]:
+            part_work()
+            if stages:
+                pl.when(g >= 1)(stages.pop(0))
+    for stage in stages:
+        pl.when(g >= 1)(stage)
+    for p in range(pairs):
+        rest4, rest1, step4, step1, step16 = work[p]
+        if not mixed:
+            for j in range(2):
+                @pl.when(g >= 1)
+                def _(j=j):
+                    early(p, j).wait_recv()
         step1(0, 0)
-        if p > 0:
-            mix_out(p - 1)
         if p == last:
             fetched(last)
         if p == 0:
             for j in range(2):
                 for b in range(1, behind + 1):
-                    @pl.when(g >= b)
-                    def _(j=j, b=b):
-                        for k in everything:
+                    for k in everything:
+                        @pl.when((g >= b) & needed(k))
+                        def _(j=j, b=b, k=k):
                             late(0, j, k, b).wait_recv()
         for u in range(4):
             if p > 0:
@@ -558,6 +693,8 @@
             step4(u, 0)
             lax.fori_loop(0, 4, lambda n, _, u=u: step16(4 * u + n, 0), 0, unroll=4)
             send_back(p, u)
+            if p > 0 and u == 0:
+                mix_out(p - 1)
             if p == last and u >= 1:
                 close(u - 1)
             if p == last and u >= 2:
@@ -602,19 +739,36 @@
         for i in range(2):
             across(i).wait_send()
             twin(3, i).wait_send()
+    if mixed:
+        @pl.when(g + 1 < count)
+        def _():
+            rise().wait_send()
+
+        @pl.when(g >= 1)
+        def _():
+            ext_twin(0, 0).wait_send()
+            for k, q in firsts + seconds:
+                ext_direct(k, q).wait_send()
+                ext_twin(k, q).wait_send()
+            for i in range(2):
+                ext_across(i).wait_send()
+                ext_twin(3, i).wait_send()
     for pair in range(pairs):
         for j in range(2):
-            @pl.when(g + 1 < count)
-            def _(pair=pair, j=j):
-                early(pair, j).wait_send()
+            if not mixed:
+                @pl.when(g + 1 < count)
+                def _(pair=pair, j=j):
+                    early(pair, j).wait_send()
 
             for b in range(1, behind + 1):
-                @pl.when(g + b < count)
-                def _(pair=pair, j=j, b=b):
-                    if pair == 0:
-                        for k in everything:
-                            late(pair, j, k, b).wait_send()
-                    else:
+                if pair == 0:
+                    for k in everything:
+                        @pl.when((g + b < count) & needed(k))
+                        def _(j=j, b=b, k=k):
+                            late(0, j, k, b).wait_send()
+                else:
+                    @pl.when(g + b < count)
+                    def _(pair=pair, j=j, b=b):
                         for u in range(4):
                             part_of(pair, j, u, b).wait_send()
 
@@ -634,7 +788,10 @@
     share = rows // n_tp
     f32, bf16 = jnp.float32, jnp.bfloat16
     dma = pltpu.SemaphoreType.DMA
-    state = pltpu.VMEM((all_rows, LANES), f32)
+    mixed = behind == 1 and group == 4
+    extra = pltpu.VMEM((rows, depth) if mixed else (16, LANES), bf16)
+    small = pltpu.VMEM((rows, LANES) if mixed else (8, LANES), f32)
+    state = pltpu.VMEM((pairs, all_rows, LANES), f32)
     weight = pltpu.VMEM((depth, part), bf16)
     table = pltpu.VMEM((all_rows, LANES), f32)
     ring = pltpu.VMEM((pairs, SPAN + all_rows, LANES), bf16)
@@ -651,12 +808,12 @@
         in_specs=[ANY, vmem, vmem, ANY, ANY, ANY, ANY, vmem],
         out_specs=(vmem, vmem),
         scratch_shapes=[
-            pltpu.VMEM((rows, depth), bf16), pltpu.VMEM((all_rows, depth), bf16),
-            weight, weight, weight, pltpu.VMEM((pairs, group * LANES, depth), bf16), table, table,
+            pltpu.VMEM((rows, depth), bf16), pltpu.VMEM((all_rows, depth), bf16), extra,
+            weight, weight, weight, pltpu.VMEM((pairs, group * LANES, depth), bf16), table, table, small, small,
             pltpu.VMEM((pairs, rows, LANES), f32),
             pltpu.VMEM((pairs, all_rows, LANES), bf16), ring, ring,
             pltpu.VMEM((pairs, WIDE, steps, LANES), bf16), woven, woven,
-            state, state, state, state, state, state, state,
+            state, state, state, state, state, state, table,
             pltpu.VMEM((2, SPAN, 2 * SPAN), f32),
             pltpu.VMEM((2, SPAN, 2 * SPAN), f32),
             pltpu.VMEM((steps, steps + SPAN), f32),
@@ -668,6 +825,7 @@
             dma((4 + pairs * group,)),
             dma((2, near)), dma((2, near)), dma((2, 2, count)), dma((2, 2, count)),
             dma((2, 2)), dma((2, 2)), dma((2,)), dma((2,)), dma((3, 2)), dma((3, 2)),
+            dma((1,)), dma((1,)), dma((2, 2)), dma((2, 2)), dma((2,)), dma((2,)), dma((4, 2)), dma((4, 2)),
             dma((pairs, 2)), dma((pairs, 2)),
             dma((pairs, 2, behind, 4)), dma((pairs, 2, behind, 4)),
             dma((pairs, near, 4)), dma((pairs, near, 4)), dma((pairs, near)), dma((pairs, near)),

time: 108 us -> 103 us (0.954)
  the two profiles are of different devices: /device:TPU:9 before, /device:TPU:25 now
where the time goes in v5:
time: 103 us; the launch traced here: 102 us
  Pallas kernels  97.3 us (94%)
  local copies, waits for them, and re-layouts  3.68 us (4%)
    pallas_call x1, Pallas kernels, layer(): pl.pallas_call(functools.partial(layer_kernel, n_sp, n_tp, group, behind)...  97.3 us
    unnamed x2, local copies, waits for them, and re-layouts  3.68 us

profile of v5, /device:TPU:25, one launch (start us, length us, event | category | flops | bytes accessed | tf_op | source)
XLA Modules:
  0.0 102.3 jit_solution(13950038255818300826)
XLA Ops:
  0.6 0.6 maximum_bitcast_fusion.freq_ref
  1.2 97.3 %layer_core.1 = (bf16[256,2048]{1,0:T(8,128)(2,1)}, f32[16,512]{1,0:T(8,128)}) custom-call(bf16[512,2048]{1,0:T(8,128)(2,1)} %hid_ref.1, f32[1,2048]{1,0:T(1,128)} %bitcast.4, f32[1,128]{1,0:T(1,128)} %maximum_bitcast_fusion.freq_ref, bf16[2048,1024]{1,0:T(8,128)(2,1)} %wq_ref.1, bf16[128,1024]{1,0:T(8,128)(2,1)} %wk_ref.1, bf16[128,1024]{1,0:T(8,128)(2,1)} %wv_ref.1, ...), custom_call_target="tpu_custom_call" | custom-call | tf_op jit(solution)/shard_map/layer_core/pallas_call | solution.py:802
  98.6 2.3 %copy.11 = bf16[256,2048]{1,0:T(8,128)(2,1)} copy(bf16[256,2048]{1,0:T(8,128)(2,1)} %get-tuple-element.4) | data formatting | bytes 2097152
  100.9 1.4 %copy.12 = f32[16,512]{1,0:T(8,128)} copy(f32[16,512]{1,0:T(8,128)} %get-tuple-element.5) | data formatting | bytes 65536
  (1 shorter events, 0.0 us)

commit v6 on v5

--- a/solution.py
+++ b/solution.py
@@ -2,6 +2,7 @@
 
 import jax
 import jax.numpy as jnp
+import numpy as np
 from jax import lax
 from jax.experimental import pallas as pl
 from jax.experimental.pallas import tpu as pltpu
@@ -48,7 +49,7 @@
     qn_all, kw_all, vw_all, qr_all, kx_all, vx_all,
     acc1_all, m1_all, l1_all, acc4_all, m4_all, l4_all, wide, b1, b4, b16,
     att, att_in, lw, lw_in, total, mix, keep, snd, rcv, final,
-    local, near_s, near_r, line_s, line_r, dir_s, dir_r, across_s, across_r, twin_s, twin_r,
+    local, own_s, own_r, near_s, near_r, line_s, line_r, dir_s, dir_r, across_s, across_r, twin_s, twin_r,
     rise_s, rise_r, edir_s, edir_r, eacross_s, eacross_r, etwin_s, etwin_r,
     early_s, early_r, late_s, late_r, back_s, back_r, level_s, level_r, swap_s, swap_r,
 ):
@@ -160,6 +161,11 @@
         slot = ref.at[pl.ds(pl.multiple_of(off * group * w_rows, group * w_rows), group * w_rows)]
         return remote(slot, slot, line_s.at[way, j, d - 1], line_r.at[way, j, d], ((up, down)[way], t))
 
+    def line_own(way, j, k):
+        at = pl.multiple_of((base + flip(c, k)) * w_rows, w_rows)
+        slot = (wk, wv)[j].at[pl.ds(at, w_rows)]
+        return remote(slot, slot, own_s.at[way, j, k], own_r.at[way, j, k], ((up, down)[way], t))
+
     def has_in(way, d):
         return g >= d if way == 0 else g + d < count
 
@@ -168,11 +174,20 @@
             return (g >= d) & (g + 1 < count)
         return (g + d < count) & (g >= 1)
 
+    def own_on(j, k):
+        for way in range(2):
+            @pl.when(has_out(way, 0))
+            def _(way=way):
+                line_own(way, j, k).start()
+
     def pass_on(j, d):
         for way in range(2):
-            if not (isinstance(d, int) and d == 0):
-                @pl.when(has_in(way, d))
-                def _(way=way):
+            @pl.when(has_in(way, d))
+            def _(way=way):
+                if isinstance(d, int) and d == 1:
+                    for k in [0] + masks:
+                        line_own(way, j, k).wait_recv()
+                else:
                     line_in(way, j, d).wait_recv()
 
             if not (isinstance(d, int) and d == count - 1):
@@ -184,7 +199,11 @@
         for way in range(2):
             @pl.when(has_out(way, d))
             def _(way=way):
-                line(way, j, d).wait_send()
+                if isinstance(d, int) and d == 0:
+                    for k in [0] + masks:
+                        line_own(way, j, k).wait_send()
+                else:
+                    line(way, j, d).wait_send()
 
     def piece(block, side, q):
         return nrm.at[pl.ds(pl.multiple_of(block * rows + side * (2 * quarter) + q * quarter, quarter), quarter)]
@@ -234,6 +253,10 @@
     for j in range(2):
         for k in masks:
             near(k, j).start()
+    kept[2].wait()
+    own_on(0, 0)
+    kept[3].wait()
+    own_on(1, 0)
     firsts = {4: [(1, 0), (2, 1)], 2: [(1, 0)], 1: []}[group]
     seconds = {4: [(1, 1), (2, 0)], 2: [(1, 1)], 1: []}[group]
     thirds = {4: [(3, 0), (3, 1)], 2: [], 1: []}[group]
@@ -327,11 +350,13 @@
     for j in range(2):
         for k in masks:
             near(k, j).wait_recv()
-        kept[2 + j].wait()
-        pass_on(j, 0)
+            own_on(j, k)
 
     kept[1].wait()
     project(0, 0)
+    if count > 1:
+        for j in range(2):
+            pass_on(j, 1)
 
     for k, q in firsts:
         direct(k, q).wait_recv()
@@ -340,15 +365,12 @@
             if k == 1:
                 direct(2, 0).start()
         twin(k, q).start()
-    if count > 1:
+    if count > 2:
         for j in range(2):
-            pass_on(j, 1)
+            pass_on(j, 2)
     for k, q in seconds[:1]:
         direct(k, q).wait_recv()
         twin(k, q).start()
-    if count > 2:
-        for j in range(2):
-            pass_on(j, 2)
     for k in masks[:1]:
         for q in range(2):
             twin(k, q).wait_recv()
@@ -414,6 +436,99 @@
                 send_late(0, j, k - 1)
             elif j == 1:
                 send_late(0, 0, everything[:2][-1])
+    skip16 = behind * steps - SPAN
+
+    def tile(q, k, v, bias):
+        n = q.shape[0]
+        low = lax.broadcasted_iota(jnp.int32, (n, LANES), 1) < HEAD_DIM
+        low_q = low.astype(f32).astype(bf16)
+        both = jnp.concatenate([q * low_q, q * (1 - low_q)], axis=0)
+        sc = lax.dot_general(both, k, (((1,), (1,)), ((), ())), preferred_element_type=f32)
+        sc = sc + jnp.concatenate([bias, bias], axis=0)
+        m = jnp.max(sc, axis=-1, keepdims=True)
+        e = jnp.exp(sc - m).astype(bf16)
+        o = jnp.dot(e, jnp.concatenate([v, jnp.ones_like(v)], axis=1), preferred_element_type=f32)
+        wide_m = jnp.broadcast_to(m, (2 * n, LANES))
+        return (
+            jnp.where(low, o[:n, :LANES], o[n:, :LANES]),
+            jnp.where(low, wide_m[:n], wide_m[n:]),
+            jnp.where(low, o[:n, LANES:], o[n:, LANES:]),
+        )
+
+    blocks4 = steps // 32
+    def tiles_of(p):
+        qn, kw, vw, qr, kx, vx = (ref.at[p] for ref in (qn_all, kw_all, vw_all, qr_all, kx_all, vx_all))
+        acc1, m1, l1 = (ref.at[p] for ref in (acc1_all, m1_all, l1_all))
+        acc4, m4, l4 = (ref.at[p] for ref in (acc4_all, m4_all, l4_all))
+
+        def step16(slot, _):
+            r = 4 * (slot % 4) + slot // 4
+            keys = pl.ds(skip16, steps + SPAN)
+            o16, m16, l16 = tile(qr[slot], kx[slot, keys, :], vx[slot, keys, :], b16[...])
+            apart = pl.ds(r, steps, stride=WIDE)
+            here = pl.ds(pl.multiple_of(slot * steps, steps), steps)
+            m_1, m_4 = m1[apart, :], m4[here, :]
+            top = jnp.maximum(m16, jnp.maximum(m_1, m_4))
+            e1, e4, e16 = jnp.exp(m_1 - top), jnp.exp(m_4 - top), jnp.exp(m16 - top)
+            whole = l1[apart, :] * e1 + l4[here, :] * e4 + l16 * e16
+            mixed = acc1[apart, :] * e1 + acc4[here, :] * e4 + o16 * e16
+            att[p, slot] = (mixed / whole).astype(bf16)
+            wide[apart, :] = top + jnp.log(whole)
+            return 0
+
+        def step4(r, i):
+            at = i * 32
+            low = at + behind * steps - 32
+            if not isinstance(i, int):
+                at = pl.multiple_of(at, 32)
+                low = pl.multiple_of(low, 32)
+            keys = pl.ds(low, 64)
+            got = tile(
+                jnp.concatenate([qr[4 * r + j, pl.ds(at, 32), :] for j in range(4)], axis=0),
+                jnp.concatenate([kx[4 * r + j, keys, :] for j in range(4)], axis=0),
+                jnp.concatenate([vx[4 * r + j, keys, :] for j in range(4)], axis=0),
+                b4[0 if isinstance(i, int) else 1],
+            )
+            for ref, value in zip((acc4, m4, l4), got):
+                for j in range(4):
+                    ref[pl.ds(pl.multiple_of((4 * r + j) * steps + at, 32), 32), :] = value[j * 32:(j + 1) * 32]
+            return 0
+
+        def step1(i, _):
+            at = pl.multiple_of(i * SPAN, SPAN)
+            here = pl.ds(at, SPAN)
+            keys = pl.ds(at, 2 * SPAN)
+            got = tile(qn[here, :], kw[keys, :], vw[keys, :], b1[jnp.minimum(i, 1)])
+            for ref, value in zip((acc1, m1, l1), got):
+                ref[here, :] = value
+            return 0
+
+        def rest4():
+            if blocks4 > 1:
+                lax.fori_loop(
+                    0, 4 * (blocks4 - 1),
+                    lambda idx, _: step4(idx // (blocks4 - 1), idx % (blocks4 - 1) + 1), 0, unroll=4,
+                )
+
+        halves = all_rows // SPAN // 2
+
+        def part1(side):
+            first = side * halves + 1
+            lax.fori_loop(0, halves - 1, lambda n, _: step1(first + n, 0), 0, unroll=halves - 1)
+
+        def soon1():
+            part1(lax.div(2 * c, group))
+
+        def rest1():
+            part1(1 - lax.div(2 * c, group))
+            step1(halves, 0)
+
+        return rest4, rest1, step4, step1, step16, soon1
+
+    work = [tiles_of(p) for p in range(pairs)]
+
+    for p in range(pairs):
+        work[p][5]()
     if group == 4:
         direct(2, 0).wait_recv()
         twin(2, 0).start()
@@ -459,26 +574,6 @@
                     def _(pair=pair, j=j, u=u, b=b):
                         part_of(pair, j, u, b).start()
 
-    skip16 = behind * steps - SPAN
-
-    def tile(q, k, v, bias):
-        n = q.shape[0]
-        low = lax.broadcasted_iota(jnp.int32, (n, LANES), 1) < HEAD_DIM
-        low_q = low.astype(f32).astype(bf16)
-        both = jnp.concatenate([q * low_q, q * (1 - low_q)], axis=0)
-        sc = lax.dot_general(both, k, (((1,), (1,)), ((), ())), preferred_element_type=f32)
-        sc = sc + jnp.concatenate([bias, bias], axis=0)
-        m = jnp.max(sc, axis=-1, keepdims=True)
-        e = jnp.exp(sc - m).astype(bf16)
-        o = jnp.dot(e, jnp.concatenate([v, jnp.ones_like(v)], axis=1), preferred_element_type=f32)
-        wide_m = jnp.broadcast_to(m, (2 * n, LANES))
-        return (
-            jnp.where(low, o[:n, :LANES], o[n:, :LANES]),
-            jnp.where(low, wide_m[:n], wide_m[n:]),
-            jnp.where(low, o[:n, LANES:], o[n:, LANES:]),
-        )
-
-    blocks4 = steps // 32
 
     mine = pl.ds(pl.multiple_of(c * LANES, LANES), LANES)
     own_steps = pl.ds(pl.multiple_of(c * few, few), few)
@@ -525,10 +620,9 @@
         for k in masks:
             for u in range(4):
                 back(p, k, u).wait_recv()
-        for u in range(4):
-            rows_in = att_in[p, pl.ds(4 * u, 4)].reshape(4 * few, group * LANES)
-            value = jnp.dot(rows_in, wo[p], preferred_element_type=f32)
-            total[u] = value if p == 0 else total[u] + value
+        rows_in = att_in[p].reshape(WIDE * few, group * LANES)
+        value = jnp.dot(rows_in, wo[p], preferred_element_type=f32).reshape(total.shape)
+        total[...] = value if p == 0 else total[...] + value
 
     last = pairs - 1
     thin = few // n_tp
@@ -547,19 +641,21 @@
             value = jnp.where(owner == o, mix[:, o * thin:(o + 1) * thin, :], value)
         return value.astype(bf16)
 
-    def close(u):
-        for k in masks:
-            back(last, k, u).wait_recv()
-        rows_in = att_in[last, pl.ds(4 * u, 4)].reshape(4 * few, group * LANES)
+    def close(v):
+        for u in (2 * v, 2 * v + 1):
+            for k in masks:
+                back(last, k, u).wait_recv()
+        rows_in = att_in[last, pl.ds(8 * v, 8)].reshape(8 * few, group * LANES)
         value = jnp.dot(rows_in, wo[last], preferred_element_type=f32)
         if last > 0:
-            value = value + total[u]
-        mix[...] = value.reshape(4, few, value.shape[1])
+            value = value + total[pl.ds(2 * v, 2)].reshape(value.shape)
+        mix[...] = value.reshape(8, few, value.shape[1])
         for k in range(1, n_tp):
-            snd[k - 1, u] = share_of(lax.rem(t + k, n_tp))
-        keep[u] = share_of(t)
-        for k in range(1, n_tp):
-            swap(k, u).start()
+            snd[k - 1, pl.ds(2 * v, 2)] = share_of(lax.rem(t + k, n_tp)).reshape(2, 4, thin, depth)
+        keep[pl.ds(2 * v, 2)] = share_of(t).reshape(2, 4, thin, depth)
+        for u in (2 * v, 2 * v + 1):
+            for k in range(1, n_tp):
+                swap(k, u).start()
 
     def settle(u):
         value = keep[u].astype(f32)
@@ -571,68 +667,6 @@
         for j in range(4):
             for i in range(depth // LANES):
                 final[i, pl.ds(u + 4 * j, thin, stride=WIDE), :] = value[j, :, i * LANES:(i + 1) * LANES]
-
-    def tiles_of(p):
-        qn, kw, vw, qr, kx, vx = (ref.at[p] for ref in (qn_all, kw_all, vw_all, qr_all, kx_all, vx_all))
-        acc1, m1, l1 = (ref.at[p] for ref in (acc1_all, m1_all, l1_all))
-        acc4, m4, l4 = (ref.at[p] for ref in (acc4_all, m4_all, l4_all))
-
-        def step16(slot, _):
-            r = 4 * (slot % 4) + slot // 4
-            keys = pl.ds(skip16, steps + SPAN)
-            o16, m16, l16 = tile(qr[slot], kx[slot, keys, :], vx[slot, keys, :], b16[...])
-            apart = pl.ds(r, steps, stride=WIDE)
-            here = pl.ds(pl.multiple_of(slot * steps, steps), steps)
-            m_1, m_4 = m1[apart, :], m4[here, :]
-            top = jnp.maximum(m16, jnp.maximum(m_1, m_4))
-            e1, e4, e16 = jnp.exp(m_1 - top), jnp.exp(m_4 - top), jnp.exp(m16 - top)
-            whole = l1[apart, :] * e1 + l4[here, :] * e4 + l16 * e16
-            mixed = acc1[apart, :] * e1 + acc4[here, :] * e4 + o16 * e16
-            att[p, slot] = (mixed / whole).astype(bf16)
-            wide[apart, :] = top + jnp.log(whole)
-            return 0
-
-        def step4(r, i):
-            at = i * 32
-            low = at + behind * steps - 32
-            if not isinstance(i, int):
-                at = pl.multiple_of(at, 32)
-                low = pl.multiple_of(low, 32)
-            keys = pl.ds(low, 64)
-            got = tile(
-                jnp.concatenate([qr[4 * r + j, pl.ds(at, 32), :] for j in range(4)], axis=0),
-                jnp.concatenate([kx[4 * r + j, keys, :] for j in range(4)], axis=0),
-                jnp.concatenate([vx[4 * r + j, keys, :] for j in range(4)], axis=0),
-                b4[0 if isinstance(i, int) else 1],
-            )
-            for ref, value in zip((acc4, m4, l4), got):
-                for j in range(4):
-                    ref[pl.ds(pl.multiple_of((4 * r + j) * steps + at, 32), 32), :] = value[j * 32:(j + 1) * 32]
-            return 0
-
-        def step1(i, _):
-            at = pl.multiple_of(i * SPAN, SPAN)
-            here = pl.ds(at, SPAN)
-            keys = pl.ds(at, 2 * SPAN)
-            got = tile(qn[here, :], kw[keys, :], vw[keys, :], b1[jnp.minimum(i, 1)])
-            for ref, value in zip((acc1, m1, l1), got):
-                ref[here, :] = value
-            return 0
-
-        def rest4():
-            if blocks4 > 1:
-                lax.fori_loop(
-                    0, 4 * (blocks4 - 1),
-                    lambda idx, _: step4(idx // (blocks4 - 1), idx % (blocks4 - 1) + 1), 0, unroll=4,
-                )
-
-        def rest1():
-            plains = all_rows // SPAN - 1
-            lax.fori_loop(1, plains + 1, step1, 0, unroll=max(x for x in range(1, 6) if plains % x == 0))
-
-        return rest4, rest1, step4, step1, step16
-
-    work = [tiles_of(p) for p in range(pairs)]
 
     def ext_first():
         for k, q in firsts:
@@ -667,7 +701,7 @@
     for stage in stages:
         pl.when(g >= 1)(stage)
     for p in range(pairs):
-        rest4, rest1, step4, step1, step16 = work[p]
+        rest4, rest1, step4, step1, step16, _ = work[p]
         if not mixed:
             for j in range(2):
                 @pl.when(g >= 1)
@@ -695,14 +729,15 @@
             send_back(p, u)
             if p > 0 and u == 0:
                 mix_out(p - 1)
-            if p == last and u >= 1:
-                close(u - 1)
-            if p == last and u >= 2:
-                settle(u - 2)
+            if p == last and u == 2:
+                close(0)
+            if p == last and u == 3:
+                settle(0)
+                settle(1)
         levels(p)
         send_levels(p)
 
-    close(3)
+    close(1)
     settle(2)
     heads = 2 * pairs
     for p in range(pairs):
@@ -819,10 +854,10 @@
             pltpu.VMEM((steps, steps + SPAN), f32),
             pltpu.VMEM((pairs, WIDE, steps, LANES), bf16), pltpu.VMEM((pairs, WIDE, few, group * LANES), bf16),
             pltpu.VMEM((pairs, 2, all_rows), f32), pltpu.VMEM((group, pairs, 2, rows), f32),
-            pltpu.VMEM((4, 4 * few, depth), f32), pltpu.VMEM((4, few, depth), f32),
+            pltpu.VMEM((4, 4 * few, depth), f32), pltpu.VMEM((8, few, depth), f32),
             pltpu.VMEM((4, 4, thin, depth), bf16), pieces, pieces,
             pltpu.VMEM((depth // LANES, share, LANES), f32),
-            dma((4 + pairs * group,)),
+            dma((4 + pairs * group,)), dma((2, 2, group)), dma((2, 2, group)),
             dma((2, near)), dma((2, near)), dma((2, 2, count)), dma((2, 2, count)),
             dma((2, 2)), dma((2, 2)), dma((2,)), dma((2,)), dma((3, 2)), dma((3, 2)),
             dma((1,)), dma((1,)), dma((2, 2)), dma((2, 2)), dma((2,)), dma((2,)), dma((4, 2)), dma((4, 2)),
@@ -838,6 +873,39 @@
     )(hidden, gain, freq, wq, wk, wv, wo, post)
 
 
+def place_kernel(out_ref, lw_ref, out_to, lw_to, held, held_lw, into, away):
+    count = into.shape[0] - 1
+    size = out_ref.shape[0] // count
+    spans = [pl.ds(i * size, size) for i in range(count)]
+    reads = [pltpu.make_async_copy(lw_ref, held_lw, into.at[count])]
+    reads += [pltpu.make_async_copy(out_ref.at[x], held.at[x], into.at[i]) for i, x in enumerate(spans)]
+    writes = [pltpu.make_async_copy(held_lw, lw_to, away.at[count])]
+    writes += [pltpu.make_async_copy(held.at[x], out_to.at[x], away.at[i]) for i, x in enumerate(spans)]
+    for copy in reads:
+        copy.start()
+    for read, write in zip(reads, writes):
+        read.wait()
+        write.start()
+    for write in writes:
+        write.wait()
+
+
+def place(out, levels):
+    parts = 4 if out.shape[0] % 64 == 0 else 1
+    return pl.pallas_call(
+        place_kernel,
+        out_shape=(jax.ShapeDtypeStruct(out.shape, out.dtype), jax.ShapeDtypeStruct(levels.shape, levels.dtype)),
+        in_specs=[ANY, ANY],
+        out_specs=(ANY, ANY),
+        scratch_shapes=[
+            pltpu.VMEM(out.shape, out.dtype), pltpu.VMEM(levels.shape, levels.dtype),
+            pltpu.SemaphoreType.DMA((parts + 1,)), pltpu.SemaphoreType.DMA((parts + 1,)),
+        ],
+        compiler_params=pltpu.CompilerParams(vmem_limit_bytes=62 * 1024 * 1024),
+        name="place_outputs",
+    )(out, levels)
+
+
 def body(mesh, hidden_in, pre_gain, query_proj, key_proj, value_proj, out_proj, post_gain):
     rows, depth = hidden_in.shape
     width = query_proj.shape[1]
@@ -845,12 +913,13 @@
     all_rows = rows * group
     behind = -(-(WIDE * SPAN) // all_rows)
     half_dim = HEAD_DIM // 2
-    frequency = ROPE_BASE ** (-(jnp.arange(half_dim, dtype=jnp.float32) * 2.0 / HEAD_DIM))
-    freq = jnp.concatenate([frequency] * (LANES // half_dim))[None, :]
-    return layer(
+    frequency = ROPE_BASE ** (-(np.arange(half_dim) * 2.0 / HEAD_DIM))
+    freq = jnp.asarray(np.tile(frequency, LANES // half_dim)[None, :], jnp.float32)
+    out, levels = layer(
         mesh, group, behind, hidden_in, pre_gain[None, :], freq,
         query_proj, key_proj, value_proj, out_proj, post_gain[None, :],
     )
+    return place(out, levels)
 
 
 def solution(mesh):

time: 103 us -> 95.3 us (0.925)
  the two profiles are of different devices: /device:TPU:25 before, /device:TPU:9 now
where the time goes in v6:
time: 95.3 us; the launch traced here: 94.9 us
  Pallas kernels  94.1 us (99%)
    pallas_call x1, Pallas kernels, layer(): pl.pallas_call(functools.partial(layer_kernel, n_sp, n_tp, group, behind)...  92.1 us
    pallas_call x1, Pallas kernels, place(): pl.pallas_call(place_kernel, out_shape=(jax.ShapeDtypeStruct(out.shape, o...  2.02 us

profile of v6, /device:TPU:9, one launch (start us, length us, event | category | flops | bytes accessed | tf_op | source)
XLA Modules:
  0.0 94.9 jit_solution(13646584836647467411)
XLA Ops:
  0.6 92.1 %layer_core.1 = (bf16[256,2048]{1,0:T(8,128)(2,1)}, f32[16,512]{1,0:T(8,128)}) custom-call(bf16[512,2048]{1,0:T(8,128)(2,1)} %hid_ref.1, f32[1,2048]{1,0:T(1,128)} %bitcast.2, f32[1,128]{1,0:T(1,128)} %constant.2.clone.freq_ref, bf16[2048,1024]{1,0:T(8,128)(2,1)} %wq_ref.1, bf16[128,1024]{1,0:T(8,128)(2,1)} %wk_ref.1, bf16[128,1024]{1,0:T(8,128)(2,1)} %wv_ref.1, ...), custom_call_target="tpu_custom_call" | custom-call | tf_op jit(solution)/shard_map/layer_core/pallas_call | solution.py:837
  92.7 2.0 %place_outputs.1 = (bf16[256,2048]{1,0:T(8,128)(2,1)}, f32[16,512]{1,0:T(8,128)}) custom-call(bf16[256,2048]{1,0:T(8,128)(2,1)} %get-tuple-element.4.out_ref, f32[16,512]{1,0:T(8,128)} %get-tuple-element.5.lw_ref), custom_call_target="tpu_custom_call" | custom-call | tf_op jit(solution)/shard_map/place_outputs/pallas_call | solution.py:895

commit v7 on v6

--- a/solution.py
+++ b/solution.py
@@ -301,10 +301,18 @@
 
     front = lax.rem(lax.broadcasted_iota(jnp.int32, (rows, LANES), 1), HEAD_DIM) < HEAD_DIM // 2
 
-    def project(k, j):
+    def project(*items):
+        outs = [
+            jnp.dot(nrm[pl.ds(pl.multiple_of(block_of(k), rows), rows), :], (wq, wk, wv)[j][...],
+                    preferred_element_type=f32)
+            for k, j in items
+        ]
+        for n, (k, j) in enumerate(items):
+            place_rows(k, j, outs[n], scr.at[n])
+
+    def place_rows(k, j, out, scr):
         row = pl.multiple_of(block_of(k), rows)
         here = pl.ds(row, rows)
-        out = jnp.dot(nrm[here, :], (wq, wk, wv)[j][...], preferred_element_type=f32)
         nat = (qn_all, kw_all, vw_all)[j]
         res = (qr_all, kx_all, vx_all)[j]
         skip = 0 if j == 0 else SPAN
@@ -341,11 +349,11 @@
                 )
                 u = u * cos_e[...] + swapped * sin_e[...]
             nat[i, pl.ds(0, SPAN), :] = u[rows - SPAN:].astype(bf16)
-            scr[i] = u
+            scr[0, i] = u
         for i in range(pairs):
             for r in range(WIDE):
                 slot = 4 * (r % 4) + r // 4
-                res[i, slot, pl.ds(end_steps, few), :] = scr[i, pl.ds(r, few, stride=WIDE), :].astype(bf16)
+                res[i, slot, pl.ds(end_steps, few), :] = scr[0, i, pl.ds(r, few, stride=WIDE), :].astype(bf16)
 
     for j in range(2):
         for k in masks:
@@ -353,7 +361,7 @@
             own_on(j, k)
 
     kept[1].wait()
-    project(0, 0)
+    project((0, 0))
     if count > 1:
         for j in range(2):
             pass_on(j, 1)
@@ -374,7 +382,7 @@
     for k in masks[:1]:
         for q in range(2):
             twin(k, q).wait_recv()
-        project(k, 0)
+        project((k, 0))
     if group == 4:
         twin(2, 1).wait_recv()
         if mixed:
@@ -422,20 +430,22 @@
         def _():
             early(pair, j).start()
 
-    for j in range(2):
-        far(j)
-        if group == 4 and j == 0:
-            twin(3, 0).wait_recv()
-            if mixed:
-                @pl.when((c == 0) & (g + 1 < count))
-                def _():
-                    rise().start()
-        for i, k in enumerate(everything[:2]):
-            project(k, 1 + j)
-            if i > 0:
-                send_late(0, j, k - 1)
-            elif j == 1:
-                send_late(0, 0, everything[:2][-1])
+    far(0)
+    if group == 4:
+        twin(3, 0).wait_recv()
+        if mixed:
+            @pl.when((c == 0) & (g + 1 < count))
+            def _():
+                rise().start()
+    ready = everything[:2]
+    for k in ready:
+        project((k, 1))
+        if k > 0:
+            send_late(0, 0, k - 1)
+    far(1)
+    project(*[(k, 2) for k in ready])
+    send_late(0, 0, ready[-1])
+
     skip16 = behind * steps - SPAN
 
     def tile(q, k, v, bias):
@@ -529,28 +539,24 @@
 
     for p in range(pairs):
         work[p][5]()
+    for k in ready:
+        send_late(0, 1, k)
     if group == 4:
         direct(2, 0).wait_recv()
         twin(2, 0).start()
         across(1).wait_recv()
         twin(3, 1).start()
-        send_late(0, 1, 1)
         twin(2, 0).wait_recv()
-        project(2, 1)
-        project(2, 2)
+        project((2, 1), (2, 2))
         if mixed:
             pl.when(g >= 1)(share_rise)
+        twin(3, 1).wait_recv()
+        project((3, 1), (3, 2))
         send_late(0, 0, 2)
-        twin(3, 1).wait_recv()
-        project(3, 1)
         send_late(0, 1, 2)
-        project(3, 2)
+        project((2, 0), (3, 0))
         send_late(0, 0, 3)
-        project(2, 0)
-        project(3, 0)
         send_late(0, 1, 3)
-    else:
-        send_late(0, 1, everything[-1])
     if not mixed:
         for j in range(2):
             send_early(0, j)
@@ -683,6 +689,8 @@
         for k, q in thirds:
             ext_across(q).wait_recv()
             ext_twin(k, q).start()
+
+    def ext_last():
         ext_twin(0, 0).wait_recv()
         for k in masks:
             for q in range(2):
@@ -692,7 +700,7 @@
 
     stages = []
     if mixed:
-        stages = [ext_first, ext_second, ext_third]
+        stages = [ext_first, ext_second, ext_third, ext_last]
     for p in range(pairs):
         for part_work in work[p][:2]:
             part_work()
@@ -845,7 +853,7 @@
         scratch_shapes=[
             pltpu.VMEM((rows, depth), bf16), pltpu.VMEM((all_rows, depth), bf16), extra,
             weight, weight, weight, pltpu.VMEM((pairs, group * LANES, depth), bf16), table, table, small, small,
-            pltpu.VMEM((pairs, rows, LANES), f32),
+            pltpu.VMEM((2, pairs, rows, LANES), f32),
             pltpu.VMEM((pairs, all_rows, LANES), bf16), ring, ring,
             pltpu.VMEM((pairs, WIDE, steps, LANES), bf16), woven, woven,
             state, state, state, state, state, state, table,

time: 95.3 us -> 95.3 us (level)
  no operation moved by 1% of the time
where the time goes in v7:
time: 95.3 us; the launch traced here: 94.5 us
  Pallas kernels  93.6 us (98%)
    pallas_call x1, Pallas kernels, layer(): pl.pallas_call(functools.partial(layer_kernel, n_sp, n_tp, group, behind)...  91.6 us
    pallas_call x1, Pallas kernels, place(): pl.pallas_call(place_kernel, out_shape=(jax.ShapeDtypeStruct(out.shape, o...  2.02 us

profile of v7, /device:TPU:9, one launch (start us, length us, event | category | flops | bytes accessed | tf_op | source)
XLA Modules:
  0.0 94.5 jit_solution(6396357250236424225)
XLA Ops:
  0.6 91.6 %layer_core.1 = (bf16[256,2048]{1,0:T(8,128)(2,1)}, f32[16,512]{1,0:T(8,128)}) custom-call(bf16[512,2048]{1,0:T(8,128)(2,1)} %hid_ref.1, f32[1,2048]{1,0:T(1,128)} %bitcast.2, f32[1,128]{1,0:T(1,128)} %constant.2.clone.freq_ref, bf16[2048,1024]{1,0:T(8,128)(2,1)} %wq_ref.1, bf16[128,1024]{1,0:T(8,128)(2,1)} %wk_ref.1, bf16[128,1024]{1,0:T(8,128)(2,1)} %wv_ref.1, ...), custom_call_target="tpu_custom_call" | custom-call | tf_op jit(solution)/shard_map/layer_core/pallas_call | solution.py:845
  92.3 2.0 %place_outputs.1 = (bf16[256,2048]{1,0:T(8,128)(2,1)}, f32[16,512]{1,0:T(8,128)}) custom-call(bf16[256,2048]{1,0:T(8,128)(2,1)} %get-tuple-element.4.out_ref, f32[16,512]{1,0:T(8,128)} %get-tuple-element.5.lw_ref), custom_call_target="tpu_custom_call" | custom-call | tf_op jit(solution)/shard_map/place_outputs/pallas_call | solution.py:903
